TPU v7x, 512 devices: a whole 4x8x8 slice. The times are simulated.
512 devices in a mesh: fs: 64 (over z, y), tp: 8 (over x, core).
Axes of the slice: x: 4, y: 8, z: 8, core: 2. Of those that a mesh axis runs over, the one named last changes fastest.
Arguments:
- late_input: bfloat16 [8192, 2048], P('fs', 'tp'), may hold values from -6 to 6
- up_weight: bfloat16 [2048, 4096], P('tp', 'fs'), may hold values from -0.125 to 0.125
- down_weight: bfloat16 [4096, 2048], P('fs', 'tp'), may hold values from -0.09375 to 0.09375
- early_input: bfloat16 [8192, 2048], P('fs', 'tp'), may hold values from -6 to 6
- early_pre: bfloat16 [8192, 4096], P('fs'), may hold values from -6 to 6
- cotangent: bfloat16 [8192, 2048], P('fs', 'tp'), may hold values from -16 to 16
- up_sum: float32 [2048, 4096], P('tp', 'fs'), may hold values from -24 to 24
- down_sum: float32 [4096, 2048], P('fs', 'tp'), may hold values from -24 to 24
Outputs:
- late_pre: bfloat16 [8192, 4096], P('fs')
- late_out: bfloat16 [8192, 2048], P('fs', 'tp')
- input_grad: bfloat16 [8192, 2048], P('fs', 'tp')
- up_total: float32 [2048, 4096], P('tp', 'fs')
- down_total: float32 [4096, 2048], P('fs', 'tp')
All inputs are finite; a program needn't handle non-finite values.
Results may differ from a plain program's by a relative error of at most 0.025.
Values may be sent and summed in bfloat16 or wider, within the bound.
A program may use at most 128 MiB of HBM per device.

v0:
```python
import jax
import jax.numpy as jnp
from jax import lax
from jax.sharding import Mesh
from jax.sharding import PartitionSpec as P

FS = ("fs_0", "fs_1")


def gathered_total(shard, axis):
    parts = lax.all_gather(shard, axis).astype(jnp.float32)
    return parts.sum(axis=0)


def own_rows(so_far, axes):
    for axis in axes:
        so_far = lax.psum_scatter(so_far, axis, scatter_dimension=0, tiled=True)
    return so_far


def contract_rows(left, right):
    return lax.dot_general(
        left, right, (((0,), (0,)), ((), ())), preferred_element_type=jnp.float32
    )


def contract_cols(left, right):
    return lax.dot_general(
        left, right, (((1,), (1,)), ((), ())), preferred_element_type=jnp.float32
    )


def body(late_input, up_weight, down_weight, early_input, early_pre, cotangent, up_sum, down_sum):
    up_gathered = lax.all_gather(up_weight, FS, axis=1, tiled=True)
    down_gathered = lax.all_gather(down_weight, FS, axis=0, tiled=True)
    pre_terms = jnp.dot(late_input, up_gathered, preferred_element_type=jnp.float32)
    pre_summed = gathered_total(pre_terms.astype(jnp.bfloat16), "tp").astype(jnp.float32)
    late_pre = pre_summed.astype(jnp.bfloat16)
    late_hidden = jnp.square(jax.nn.relu(late_pre.astype(jnp.float32))).astype(jnp.bfloat16)
    early_float = early_pre.astype(jnp.float32)
    early_hidden = jnp.square(jax.nn.relu(early_float)).astype(jnp.bfloat16)
    late_out = jnp.dot(late_hidden, down_gathered, preferred_element_type=jnp.float32).astype(
        jnp.bfloat16
    )
    grad_terms = contract_cols(cotangent, down_gathered)
    hidden_grad = gathered_total(grad_terms.astype(jnp.bfloat16), "tp").astype(jnp.float32)
    pre_grad = (hidden_grad * 2.0 * jax.nn.relu(early_float)).astype(jnp.bfloat16)
    input_grad = contract_cols(pre_grad, up_gathered).astype(jnp.bfloat16)
    grad_local = lax.all_to_all(pre_grad, FS, split_axis=1, concat_axis=0, tiled=True)
    up_grad = contract_rows(lax.all_gather(early_input, FS, axis=0, tiled=True), grad_local)
    up_total = up_sum + up_grad
    down_grad = own_rows(contract_rows(early_hidden, cotangent), FS)
    down_total = down_sum + down_grad
    return (late_pre, late_out, input_grad, up_total, down_total)


def solution(mesh):
    split = Mesh(mesh.devices.reshape(8, 8, mesh.shape["tp"]), ("fs_0", "fs_1", "tp"))
    placed = (
        P(FS, "tp"),
        P("tp", FS),
        P(FS, "tp"),
        P(FS, "tp"),
        P(FS, None),
        P(FS, "tp"),
        P("tp", FS),
        P(FS, "tp"),
    )
    return jax.shard_map(
        body,
        mesh=split,
        in_specs=placed,
        out_specs=(P(FS, None), P(FS, "tp"), P(FS, "tp"), P("tp", FS), P(FS, "tp")),
        check_vma=False,
    )
```

profile of v0, /device:TPU:1, one launch (start us, length us, event | category | flops | bytes accessed | tf_op | source)
XLA Modules:
  0.0 411.1 jit_solution(17327344246205105072)
XLA Ops:
  8.0 0.0 all-gather.10.cloned.1.call-start
  8.1 0.7 all-gather.10.cloned.1.call-update
  8.7 0.0 reduce-scatter.3.cloned.1.call-start
  8.8 0.0 copy-done
  8.8 3.9 fusion.1
  12.8 0.0 all-gather.8.cloned.1.call-start
  12.8 0.7 all-gather.8.cloned.1.call-update
  13.6 0.0 all-gather.16.cloned.1.call-start
  13.6 101.1 %all-gather.10.cloned.1.call-done = bf16[4096,256]{1,0:T(8,128)(2,1)} async-done(((bf16[64,256]{1,0:T(8,128)(2,1)}), bf16[4096,256]{1,0:T(8,128)(2,1)}) %all-gather.10.cloned.1.call-update) | async-done | bytes 2097168 | tf_op jit(solution)/shard_map/all_gather | solution.py:35
  114.7 3.5 convolution_convert_fusion
  118.2 0.0 reduce-scatter.5.cloned.1.call-start
  118.2 0.5 reduce-scatter.5.cloned.1.call-update
  118.7 0.0 all-gather.14.cloned.1.call-start
  118.8 79.3 %all-gather.8.cloned.1.call-done = bf16[256,4096]{0,1:T(8,128)(2,1)} async-done(((bf16[256,64]{0,1:T(8,128)(2,1)}), bf16[256,4096]{0,1:T(8,128)(2,1)}) %all-gather.8.cloned.1.call-update) | async-done | bytes 2097168 | tf_op jit(solution)/shard_map/all_gather | solution.py:34
  198.1 3.4 convolution_convert_fusion.1
  201.5 0.0 all-gather.12.cloned.1.call-start
  201.5 0.5 all-gather.12.cloned.1.call-update
  202.1 54.7 %all-gather.16.cloned.1.call-done = bf16[1024,4096]{1,0:T(8,128)(2,1)} async-done(((bf16[128,4096]{1,0:T(8,128)(2,1)}), bf16[1024,4096]{1,0:T(8,128)(2,1)}) %all-gather.16.cloned.1.call-update) | async-done | bytes 8388624 | tf_op jit(solution)/shard_map/all_gather | solution.py:11
  256.7 5.1 %convert_reduce_fusion = f32[128,4096]{1,0:T(8,128)S(1)} fusion(bf16[8,128,4096]{2,1,0:T(8,128)(2,1)} %bitcast.25), kind=kLoop, calls=%fused_computation | loop fusion | flops 7864320 | bytes 10485760 | tf_op jit(solution)/shard_map/reduce_sum | solution.py:12
  261.9 0.3 multiply_convert_fusion.1
  262.2 1.3 copy.16
  263.6 13.3 %all-to-all-start = ((bf16[128,64,64]{0,2,1:T(8,128)(2,1)}), bf16[128,64,64]{0,2,1:T(8,128)(2,1)}, u32[]{:S(2)}, u32[]{:S(2)}) async-start(bf16[128,64,64]{0,2,1:T(8,128)(2,1)} %bitcast.2), calls=%async_computation | async-start | bytes 2097152 | tf_op jit(solution)/shard_map/all_to_all | solution.py:49
  276.8 0.0 reduce-scatter.5.cloned.1.call-done
  276.9 1.5 add.11
  278.4 36.2 %all-gather.14.cloned.1.call-done = bf16[1024,4096]{1,0:T(8,128)(2,1)} async-done(((bf16[128,4096]{1,0:T(8,128)(2,1)}), bf16[1024,4096]{1,0:T(8,128)(2,1)}) %all-gather.14.cloned.1.call-update) | async-done | bytes 8388624 | tf_op jit(solution)/shard_map/all_gather | solution.py:11
  314.6 6.2 %reduce_sum.21 = bf16[128,4096]{1,0:T(8,128)(2,1)} reduce(bf16[8,128,4096]{2,1,0:T(8,128)(2,1)} %bitcast.26, bf16[]{:T(256)} %constant.7.clone.1), dimensions={0}, to_apply=%region_0.0 | reduce | flops 3670016 | bytes 9437186 | tf_op jit(solution)/shard_map/reduce_sum | solution.py:12
  320.8 1.1 convolution_convert_fusion.2
  321.9 0.5 copy-done.3
  322.4 0.3 copy-done.4
  322.7 1.1 convolution_convert_fusion.3
  323.7 76.3 %all-gather.12.cloned.1.call-done = bf16[8192,256]{1,0:T(8,128)(2,1)} async-done(((bf16[128,256]{1,0:T(8,128)(2,1)}), bf16[8192,256]{1,0:T(8,128)(2,1)}) %all-gather.12.cloned.1.call-update) | async-done | bytes 4194320 | tf_op jit(solution)/shard_map/all_gather | solution.py:50
  400.0 4.0 fusion
  (18 shorter events, 0.1 us)
Async XLA Ops:
  8.0 0.8 copy-start
  8.0 106.7 %all-gather.10.cloned.1.call-start = ((), (), s32[]{:S(2)}) async-start(), calls=%async_computation.4 | async-start | bytes 2129920 | tf_op jit(solution)/shard_map/all_gather | solution.py:35
  8.7 109.5 %reduce-scatter.3.cloned.1.call-start = ((), (), s32[]{:S(2)}) async-start(), calls=%async_computation.6 | async-start | bytes 4718592 | tf_op jit(solution)/shard_map/reduce_scatter | solution.py:17
  12.8 185.3 %all-gather.8.cloned.1.call-start = ((), (), s32[]{:S(2)}) async-start(), calls=%async_computation.3 | async-start | bytes 2129920 | tf_op jit(solution)/shard_map/all_gather | solution.py:34
  13.5 184.5 %copy-start.6 = (bf16[128,256]{1,0:T(8,128)(2,1)S(1)}, bf16[128,256]{1,0:T(8,128)(2,1)}, u32[]{:S(2)}) copy-start(bf16[128,256]{1,0:T(8,128)(2,1)} %param.8) | copy-start | bytes 196612
  13.6 243.2 %all-gather.16.cloned.1.call-start = ((), (), s32[]{:S(2)}) async-start(), calls=%async_computation.9 | async-start | bytes 9437184 | tf_op jit(solution)/shard_map/all_gather | solution.py:11
  118.2 158.7 %reduce-scatter.5.cloned.1.call-start = ((), (), s32[]{:S(2)}) async-start(), calls=%async_computation.7 | async-start | bytes 589824 | tf_op jit(solution)/shard_map/reduce_scatter | solution.py:17
  118.7 195.8 %all-gather.14.cloned.1.call-start = ((), (), s32[]{:S(2)}) async-start(), calls=%async_computation.8 | async-start | bytes 9437184 | tf_op jit(solution)/shard_map/all_gather | solution.py:11
  201.5 198.5 %all-gather.12.cloned.1.call-start = ((), (), s32[]{:S(2)}) async-start(), calls=%async_computation.5 | async-start | bytes 4259840 | tf_op jit(solution)/shard_map/all_gather | solution.py:50
  256.7 5.1 %copy-start.2 = (bf16[128,4096]{1,0:T(8,128)(2,1)S(1)}, bf16[128,4096]{1,0:T(8,128)(2,1)}, u32[]{:S(2)}) copy-start(bf16[128,4096]{1,0:T(8,128)(2,1)} %param.12) | copy-start | bytes 3145732
  262.2 14.7 %copy-start.7 = (f32[64,256]{1,0:T(8,128)S(1)}, f32[64,256]{1,0:T(8,128)}, u32[]{:S(2)}) copy-start(f32[64,256]{1,0:T(8,128)} %param.15) | copy-start | bytes 196612
  263.6 136.4 %all-to-all-start = ((bf16[128,64,64]{0,2,1:T(8,128)(2,1)}), bf16[128,64,64]{0,2,1:T(8,128)(2,1)}, u32[]{:S(2)}, u32[]{:S(2)}) async-start(bf16[128,64,64]{0,2,1:T(8,128)(2,1)} %bitcast.2), calls=%async_computation | async-start | bytes 2097152 | tf_op jit(solution)/shard_map/all_to_all | solution.py:49
  314.6 6.2 %copy-start.1 = (bf16[256,4096]{0,1:T(8,128)(2,1)S(1)}, bf16[256,4096]{0,1:T(8,128)(2,1)}, u32[]{:S(2)}) copy-start(bf16[256,4096]{0,1:T(8,128)(2,1)} %all-gather.8.cloned.1.call-done) | copy-start | bytes 6291460
  320.8 1.6 copy-start.3
  320.8 1.9 copy-start.4
  322.7 77.3 %copy-start.5 = (f32[256,64]{0,1:T(8,128)S(1)}, f32[256,64]{0,1:T(8,128)}, u32[]{:S(2)}) copy-start(f32[256,64]{0,1:T(8,128)} %param.14) | copy-start | bytes 196612
Sparse Core Ops, SparseCore 0:
  11.9 102.7 all-gather.9
  117.7 80.3 all-gather.7
  200.2 56.4 all-gather.15
  259.3 55.1 all-gather.13
  317.5 82.4 all-gather.11
Sparse Core Ops, SparseCore 1:
  12.9 65.2 reduce-scatter.2
  121.4 37.0 reduce-scatter.4
where the time goes:
time: 415 us; the launch traced here: 411 us
  waiting for transfers between devices  350 us (84%)
  matrix products  16.9 us (4%)
  between operations  15.3 us (4%)
  starting transfers between devices  13.6 us (3%)
  other arithmetic  13.1 us (3%)
    all_gather x1, waiting for transfers between devices, body(): down_gathered = lax.all_gather(down_weight, FS, axis=0, tiled=True)  101 us
    all_gather x2, waiting for transfers between devices, gathered_total(): parts = lax.all_gather(shard, axis).astype(jnp.float32)  90.9 us
    all_gather x1, waiting for transfers between devices, body(): up_gathered = lax.all_gather(up_weight, FS, axis=1, tiled=True)  79.3 us
    all_gather x1, waiting for transfers between devices, body(): lax.all_gather(early_input, FS, axis=0, tiled=True)  76.3 us
    all_to_all x1, starting transfers between devices, body(): lax.all_to_all(pre_grad, FS, split_axis=1, concat_axis=0, tiled=True)  13.3 us
    reduce_sum x2, other arithmetic, gathered_total(): return parts.sum(axis=0)  11.3 us
  transfers between devices with their start and end apart: 8, of which 5 were waited for; matrix products, arithmetic and copies ran while one was open for 7% of the time, Pallas kernels for 0%

commit v1 on v0

v1 whole, which is shorter than its diff:
```python
import jax
import jax.numpy as jnp
from jax import lax
from jax.experimental import pallas as pl
from jax.experimental.pallas import tpu as pltpu
from jax.sharding import Mesh
from jax.sharding import PartitionSpec as P

FS = ("z", "y")
TP = ("x", "c")
MESH = pl.DeviceIdType.MESH
F32 = jnp.float32
BF16 = jnp.bfloat16
BLOCK_AXIS = ("z", "y")
SUB_AXIS = ("y", "z")


def nn(left, right):
    return lax.dot_general(left, right, (((1,), (0,)), ((), ())), preferred_element_type=F32)


def tn(left, right):
    return lax.dot_general(left, right, (((0,), (0,)), ((), ())), preferred_element_type=F32)


def square_relu(value):
    return jnp.square(jnp.maximum(value.astype(F32), 0.0)).astype(BF16)


def kernel(
    late_in, up_t, down, early_in, early_pre, cot, up_sum, down_sum,
    late_pre_o, late_out_o, input_grad_o, up_total_o, down_total_o,
    weights, grads, ring_in, last_in, early_t, cot_t, late_t, part, pair_in, pair_sum, x_in, full, acc,
    own_sem, ag1_s, ag1_r, ag2_s, ag2_r, rs1_s, rs1_r, rs2_s, rs2_r,
    pair_s, pair_r, xr_s, xr_r, xg_s, xg_r, cg_s, cg_r, fw_s, fw_r,
):
    iz, iy, ix, ic = (lax.axis_index(name) for name in ("z", "y", "x", "c"))
    place = (iz, iy)
    sub_place = (iy, iz)
    shards = (down, up_t)
    sent = []

    def up_by(value, step, size=8):
        return lax.rem(value + (step % size), size)

    def remote(src, dst, send_sem, recv_sem, axis, index):
        return pltpu.make_async_remote_copy(
            src_ref=src, dst_ref=dst, send_sem=send_sem, recv_sem=recv_sem,
            device_id={axis: index}, device_id_type=MESH,
        )

    def send(*args):
        copy = remote(*args)
        copy.start()
        sent.append(copy)

    barrier = pltpu.get_barrier_semaphore()
    for axis, me, size in (("y", iy, 8), ("z", iz, 8), ("x", ix, 4), ("c", ic, 2)):
        for step in range(1, size):
            pl.semaphore_signal(
                barrier, inc=1, device_id={axis: up_by(me, step, size)}, device_id_type=MESH
            )
    pl.semaphore_wait(barrier, 18)

    own = []

    def ag1_send(w):
        for h in range(2):
            rows = shards[w].at[pl.ds(32 * h, 32), :]
            target = weights.at[w, h, place[h], sub_place[h]]
            copy = pltpu.make_async_copy(rows, target, own_sem.at[w, h])
            copy.start()
            own.append(copy)
            for step in (4, 3, 5, 2, 6, 1, 7):
                send(
                    rows, target, ag1_s.at[w, h, step - 1], ag1_r.at[w, h, step - 1],
                    SUB_AXIS[h], up_by(sub_place[h], step),
                )

    def ag1_wait(w):
        for h in range(2):
            own[2 * w + h].wait()
            for step in range(1, 8):
                target = weights.at[w, h, place[h], up_by(sub_place[h], -step)]
                remote(
                    target, target, ag1_s.at[w, h, step - 1], ag1_r.at[w, h, step - 1],
                    SUB_AXIS[h], up_by(sub_place[h], -step),
                ).wait_recv()

    def ag2_piece(w, h, way, step, part_at, arriving):
        sign = 1 - 2 * way
        away = -sign * (step if arriving else step - 1)
        ref = weights.at[w, h, up_by(place[h], away), pl.ds(4 * part_at, 4)]
        at = (w, h, way, step - 1, part_at)
        return ref, ref, ag2_s.at[at], ag2_r.at[at], BLOCK_AXIS[h], up_by(place[h], sign)

    def ag2_has(step, way, part_at):
        return step < 4 or part_at == way

    def ag2_start(w):
        for part_at in range(2):
            for h in range(2):
                for way in range(2):
                    send(*ag2_piece(w, h, way, 1, part_at, False))

    def ag2_step(w, step):
        for part_at in range(2):
            for h in range(2):
                for way in range(2):
                    if ag2_has(step, way, part_at):
                        remote(*ag2_piece(w, h, way, step, part_at, True)).wait_recv()
                        if step < 4 and ag2_has(step + 1, way, part_at):
                            send(*ag2_piece(w, h, way, step + 1, part_at, False))

    def rs_send(w, h, way, step, part_at):
        sign = 1 - 2 * way
        at = (w, h, way, step - 1, part_at)
        send(
            grads.at[w, h, up_by(place[h], sign * (5 - step)), pl.ds(4 * part_at, 4)],
            ring_in.at[w, h, way, step - 1, pl.ds(4 * part_at, 4)],
            rs1_s.at[at], rs1_r.at[at], BLOCK_AXIS[h], up_by(place[h], sign),
        )

    def rs_wait(w, h, way, step, part_at):
        sign = 1 - 2 * way
        at = (w, h, way, step - 1, part_at)
        ref = ring_in.at[w, h, way, step - 1, pl.ds(4 * part_at, 4)]
        remote(ref, ref, rs1_s.at[at], rs1_r.at[at], BLOCK_AXIS[h], up_by(place[h], sign)).wait_recv()
        return ref

    def rs_start(w):
        for h in range(2):
            for way in range(2):
                rs_send(w, h, way, 1, way)
        for h in range(2):
            for way in range(2):
                rs_send(w, h, way, 2, 1 - way)

    def rs_step(w, step):
        for part_at in range(2):
            for h in range(2):
                for way in range(2):
                    if step == 1 and part_at != way:
                        continue
                    arrived = rs_wait(w, h, way, step, part_at)
                    block = up_by(place[h], (1 - 2 * way) * (4 - step))
                    mine = grads.at[w, h, block, pl.ds(4 * part_at, 4)]
                    mine[...] = (mine[...].astype(F32) + arrived[...].astype(F32)).astype(BF16)
                    rs_send(w, h, way, step + 1, part_at)

    def rs_last(w):
        for part_at in range(2):
            for h in range(2):
                mine = grads.at[w, h, place[h], pl.ds(4 * part_at, 4)]
                total = mine[...].astype(F32)
                for way in range(2):
                    total = total + rs_wait(w, h, way, 4, part_at)[...].astype(F32)
                mine[...] = total.astype(BF16)
        for h in range(2):
            for step in (4, 3, 5, 2, 6, 1, 7):
                send(
                    grads.at[w, h, place[h], up_by(sub_place[h], step)], last_in.at[w, h, step - 1],
                    rs2_s.at[w, h, step - 1], rs2_r.at[w, h, step - 1],
                    SUB_AXIS[h], up_by(sub_place[h], step),
                )

    def rs_out(w):
        base, out = ((down_sum, down_total_o), (up_sum, up_total_o))[w]
        for h in range(2):
            total = grads[w, h, place[h], sub_place[h]].astype(F32)
            for step in range(1, 8):
                ref = last_in.at[w, h, step - 1]
                remote(
                    ref, ref, rs2_s.at[w, h, step - 1], rs2_r.at[w, h, step - 1],
                    SUB_AXIS[h], up_by(sub_place[h], step),
                ).wait_recv()
                total = total + ref[...].astype(F32)
            rows = pl.ds(32 * h, 32)
            out[rows, :] = base[rows, :] + total

    def block_of(h, side, j):
        return lax.rem(iz * (1 - h) + iy * h + side * (2 * j + 1) - j + 8, 8)

    def product(a, j, sides):
        w, right = ((0, cot_t), (1, late_t))[a]

        def one(h, _):
            for side in sides:
                rows = weights[w, h, block_of(h, side, j)].reshape(256, 256)
                part[a, j, pl.ds(pl.multiple_of(h * 512 + side * 256, 256), 256), :] = nn(
                    rows, right[...]
                ).astype(BF16)
            return 0

        lax.fori_loop(0, 2, one, 0)

    other = up_by(ic, 1, 2)
    my_half = pl.multiple_of(ic * 512, 512)
    other_half = pl.multiple_of(other * 512, 512)

    def s1(a, j):
        send(
            part.at[a, j, pl.ds(other_half, 512), :], pair_in.at[a, j],
            pair_s.at[a, j], pair_r.at[a, j], "c", other,
        )

    def s2(a, j):
        ref = pair_in.at[a, j]
        remote(ref, ref, pair_s.at[a, j], pair_r.at[a, j], "c", other).wait_recv()
        pair_sum[a, j] = (
            part[a, j, pl.ds(my_half, 512), :].astype(F32) + pair_in[a, j].astype(F32)
        ).astype(BF16)
        for step in (2, 1, 3):
            target = up_by(ix, step, 4)
            rows = pl.ds(pl.multiple_of(target * 128, 128), 128)
            at = (a, j, step - 1)
            send(pair_sum.at[a, j, rows, :], x_in.at[at], xr_s.at[at], xr_r.at[at], "x", target)

    def rows_of(core, x):
        return pl.ds(pl.multiple_of(core * 512 + x * 128, 128), 128)

    def s3(a, j):
        total = pair_sum[a, j, pl.ds(pl.multiple_of(ix * 128, 128), 128), :].astype(F32)
        for step in (1, 3, 2):
            at = (a, j, step - 1)
            ref = x_in.at[at]
            remote(ref, ref, xr_s.at[at], xr_r.at[at], "x", up_by(ix, step, 4)).wait_recv()
            total = total + ref[...].astype(F32)
        mine = rows_of(ic, ix)
        if a == 0:
            block = block_of(ic, ix // 2, j)
            saved = early_t[ic, block, pl.ds(4 * lax.rem(ix, 2), 4)].reshape(128, 128)
            total = total * 2.0 * jnp.maximum(saved.astype(F32), 0.0)
        full[a, j, mine, :] = total.astype(BF16)
        ref = full.at[a, j, mine, :]
        for step in (2, 1, 3):
            at = (a, j, step - 1)
            send(ref, ref, xg_s.at[at], xg_r.at[at], "x", up_by(ix, step, 4))
        send(ref, ref, cg_s.at[a, j], cg_r.at[a, j], "c", other)

    def s4(a, j):
        for step in (1, 3, 2):
            at = (a, j, step - 1)
            source = up_by(ix, -step, 4)
            ref = full.at[a, j, rows_of(ic, source), :]
            remote(ref, ref, xg_s.at[at], xg_r.at[at], "x", source).wait_recv()
            send(ref, ref, fw_s.at[at], fw_r.at[at], "c", other)

    def s5(a, j):
        ref = full.at[a, j, rows_of(other, ix), :]
        remote(ref, ref, cg_s.at[a, j], cg_r.at[a, j], "c", other).wait_recv()
        for step in (1, 3, 2):
            at = (a, j, step - 1)
            ref = full.at[a, j, rows_of(other, up_by(ix, -step, 4)), :]
            remote(ref, ref, fw_s.at[at], fw_r.at[at], "c", other).wait_recv()

    def pieces(j, fn):
        def one(at, _):
            h, side = at // 2, lax.rem(at, 2)
            fn(h, block_of(h, side, j), pl.ds(pl.multiple_of(at * 256, 256), 256))
            return 0

        lax.fori_loop(0, 4, one, 0)

    def up_grads(j):
        def fn(h, block, rows):
            grads[1, h, block] = nn(full[0, j, rows, :], early_in[...]).astype(BF16).reshape(8, 32, 256)

        pieces(j, fn)

    def input_grads(j):
        def fn(h, block, rows):
            acc[0] += tn(full[0, j, rows, :], weights[1, h, block].reshape(256, 256))

        pieces(j, fn)

    def late_outs(j):
        def fn(h, block, rows):
            acc[1] += tn(square_relu(full[1, j, rows, :]), weights[0, h, block].reshape(256, 256))
            for sub in range(8):
                early_t[h, block, sub] = full[1, j, pl.ds(rows.start + 32 * sub, 32), :]

        pieces(j, fn)

    def turn_early(at, _):
        z, y = at // 4, 2 * lax.rem(at, 4)
        turned = early_pre[:, pl.ds(pl.multiple_of(at * 128, 128), 128)].T
        early_t[0, z, y] = turned[0:32]
        early_t[1, y, z] = turned[32:64]
        early_t[0, z, y + 1] = turned[64:96]
        early_t[1, y + 1, z] = turned[96:128]
        return 0

    def turn_late(at, _):
        z, y = at // 4, 2 * lax.rem(at, 4)
        rows = jnp.concatenate(
            [early_t[0, z, y], early_t[1, y, z], early_t[0, z, y + 1], early_t[1, y + 1, z]], axis=0
        )
        late_pre_o[:, pl.ds(pl.multiple_of(at * 128, 128), 128)] = rows.T
        return 0

    def down_grads(at, _):
        h, block = at // 8, lax.rem(at, 8)
        hidden = square_relu(early_t[h, block].reshape(256, 128))
        grads[0, h, block] = nn(hidden, cot[...]).astype(BF16).reshape(8, 32, 256)
        return 0

    ag1_send(0)
    ag1_send(1)
    cot_t[...] = cot[...].T
    late_t[...] = late_in[...].T
    acc[...] = jnp.zeros_like(acc)
    lax.fori_loop(0, 32, turn_early, 0)
    ag1_wait(0)
    ag2_start(0)
    product(0, 0, (0,))
    lax.fori_loop(0, 16, down_grads, 0)
    ag2_step(0, 1)
    product(0, 0, (1,))
    s1(0, 0)
    product(0, 1, (0,))
    s2(0, 0)
    ag2_step(0, 2)
    product(0, 1, (1,))
    s1(0, 1)
    product(0, 2, (0,))
    s2(0, 1)
    ag2_step(0, 3)
    ag1_wait(1)
    ag2_start(1)
    product(0, 2, (1,))
    s1(0, 2)
    product(0, 3, (0,))
    s3(0, 0)
    s2(0, 2)
    ag2_step(0, 4)
    product(0, 3, (1,))
    s1(0, 3)
    s3(0, 1)
    s4(0, 0)
    s2(0, 3)
    s3(0, 2)
    ag2_step(1, 1)
    s5(0, 0)
    s4(0, 1)
    up_grads(0)
    s3(0, 3)
    ag2_step(1, 2)
    s5(0, 1)
    s4(0, 2)
    up_grads(1)
    ag2_step(1, 3)
    rs_start(0)
    s5(0, 2)
    s4(0, 3)
    up_grads(2)
    s5(0, 3)
    up_grads(3)
    rs_start(1)
    ag2_step(1, 4)
    for j in range(4):
        product(1, j, (0, 1))
        s1(1, j)
    rs_step(0, 1)
    for j in range(4):
        s2(1, j)
    rs_step(1, 1)
    rs_step(0, 2)
    s3(1, 0)
    s3(1, 1)
    rs_step(1, 2)
    s3(1, 2)
    s3(1, 3)
    rs_step(0, 3)
    s4(1, 0)
    s4(1, 1)
    rs_step(1, 3)
    s4(1, 2)
    s4(1, 3)
    rs_last(0)
    for j in range(4):
        s5(1, j)
        late_outs(j)
    rs_last(1)
    for j in range(4):
        input_grads(j)
    late_out_o[...] = acc[1].astype(BF16)
    input_grad_o[...] = acc[0].astype(BF16)
    lax.fori_loop(0, 32, turn_late, 0)
    rs_out(0)
    rs_out(1)
    for copy in sent:
        copy.wait_send()


def body(late_input, up_weight, down_weight, early_input, early_pre, cotangent, up_sum, down_sum):
    vmem = pl.BlockSpec(memory_space=pltpu.VMEM)
    dma = pltpu.SemaphoreType.DMA
    outs = pl.pallas_call(
        kernel,
        out_shape=(
            jax.ShapeDtypeStruct((128, 4096), BF16),
            jax.ShapeDtypeStruct((128, 256), BF16),
            jax.ShapeDtypeStruct((128, 256), BF16),
            jax.ShapeDtypeStruct((64, 256), F32),
            jax.ShapeDtypeStruct((64, 256), F32),
        ),
        in_specs=[vmem] * 8,
        out_specs=(vmem,) * 5,
        scratch_shapes=[
            pltpu.VMEM((2, 2, 8, 8, 32, 256), BF16),
            pltpu.VMEM((2, 2, 8, 8, 32, 256), BF16),
            pltpu.VMEM((2, 2, 2, 4, 8, 32, 256), BF16),
            pltpu.VMEM((2, 2, 7, 32, 256), BF16),
            pltpu.VMEM((2, 8, 8, 32, 128), BF16),
            pltpu.VMEM((256, 128), BF16),
            pltpu.VMEM((256, 128), BF16),
            pltpu.VMEM((2, 4, 1024, 128), BF16),
            pltpu.VMEM((2, 4, 512, 128), BF16),
            pltpu.VMEM((2, 4, 512, 128), BF16),
            pltpu.VMEM((2, 4, 3, 128, 128), BF16),
            pltpu.VMEM((2, 4, 1024, 128), BF16),
            pltpu.VMEM((2, 128, 256), F32),
            dma((2, 2)),
            dma((2, 2, 7)), dma((2, 2, 7)),
            dma((2, 2, 2, 4, 2)), dma((2, 2, 2, 4, 2)),
            dma((2, 2, 2, 4, 2)), dma((2, 2, 2, 4, 2)),
            dma((2, 2, 7)), dma((2, 2, 7)),
            dma((2, 4)), dma((2, 4)),
            dma((2, 4, 3)), dma((2, 4, 3)),
            dma((2, 4, 3)), dma((2, 4, 3)),
            dma((2, 4)), dma((2, 4)),
            dma((2, 4, 3)), dma((2, 4, 3)),
        ],
        compiler_params=pltpu.CompilerParams(
            collective_id=0, has_side_effects=True, vmem_limit_bytes=60 * 1024 * 1024
        ),
        cost_estimate=pl.CostEstimate(flops=1_700_000_000, bytes_accessed=8_000_000, transcendentals=0),
    )(late_input, up_weight.T, down_weight, early_input, early_pre, cotangent, up_sum.T, down_sum)
    late_pre, late_out, input_grad, up_total, down_total = outs
    return late_pre, late_out, input_grad, up_total.T, down_total


def solution(mesh):
    split = Mesh(mesh.devices.reshape(8, 8, 4, 2), FS + TP)
    placed = (
        P(FS, TP), P(TP, FS), P(FS, TP), P(FS, TP), P(FS, None), P(FS, TP), P(TP, FS), P(FS, TP),
    )
    return jax.shard_map(
        body,
        mesh=split,
        in_specs=placed,
        out_specs=(P(FS, None), P(FS, TP), P(FS, TP), P(TP, FS), P(FS, TP)),
        check_vma=False,
    )
```

time: 415 us -> 93.2 us (0.22)
  waiting for transfers between devices: 350 us -> 0 us
  Pallas kernels: 0 us -> 86.7 us
  matrix products: 16.9 us -> 0 us
  between operations: 15.3 us -> 0.66 us
  starting transfers between devices: 13.6 us -> 0 us
  other arithmetic: 13.1 us -> 0 us
    all_gather x5 -> x0, waiting for transfers between devices: 347 us -> none  [the longest x1 101 us: body(): down_gathered = lax.all_gather(down_weight, FS, axis=0, tiled=True)]
    pallas_call x0 -> x1, Pallas kernels: none -> 86.7 us  [body(): pl.pallas_call(kernel, out_shape=(jax.ShapeDtypeStruct((128, 4096), BF16)...]
    dot_general x6 -> x0, matrix products: 16.9 us -> none  [the longest x2 7.9 us: contract_rows(): lax.dot_general(left, right, (((0,), (0,)), ((), ())), preferred_element_...]
    all_to_all x1 -> x0, starting transfers between devices: 13.3 us -> none  [body(): lax.all_to_all(pre_grad, FS, split_axis=1, concat_axis=0, tiled=True)]
    reduce_sum x2 -> x0, other arithmetic: 11.3 us -> none  [gathered_total(): return parts.sum(axis=0)]
    unnamed x16 -> x13, local copies, waits for them, and re-layouts: 0.88 us -> 5.54 us
  transfers between devices with their start and end apart: 8 -> 0, of which waited for: 5 -> 0; matrix products, arithmetic and copies ran while one was open for 7% -> 0% of each run, Pallas kernels for 0% -> 0%
where the time goes in v1:
time: 93.2 us; the launch traced here: 92.9 us
  Pallas kernels  86.7 us (93%)
  local copies, waits for them, and re-layouts  5.54 us (6%)
    pallas_call x1, Pallas kernels, body(): pl.pallas_call(kernel, out_shape=(jax.ShapeDtypeStruct((128, 4096), BF16)...  86.7 us
    unnamed x13, local copies, waits for them, and re-layouts  5.54 us

profile of v1, /device:TPU:1, one launch (start us, length us, event | category | flops | bytes accessed | tf_op | source)
XLA Modules:
  0.0 92.9 jit_solution(44865852422182847)
XLA Ops:
  0.6 86.7 %shard_map.119 = (bf16[128,4096]{1,0:T(8,128)(2,1)}, bf16[128,256]{1,0:T(8,128)(2,1)}, bf16[128,256]{1,0:T(8,128)(2,1)}, f32[64,256]{1,0:T(8,128)}, f32[64,256]{1,0:T(8,128)}) custom-call(bf16[128,256]{1,0:T(8,128)(2,1)} %late_in.1, bf16[64,256]{1,0:T(8,128)(2,1)} %bitcast.5, bf16[64,256]{1,0:T(8,128)(2,1)} %down.1, bf16[128,256]{1,0:T(8,128)(2,1)} %early_in.1, ...), custom_call_target="tpu_custom_call" | custom-call | flops 1700000000 | bytes 8000000 | tf_op jit(solution)/shard_map/pallas_call | solution.py:399
  87.4 0.0 copy-start.3
  87.4 2.3 %copy.18 = bf16[128,4096]{1,0:T(8,128)(2,1)} copy(bf16[128,4096]{1,0:T(8,128)(2,1)} %get-tuple-element.20) | data formatting | bytes 2097152
  89.7 0.0 copy-done.3
  89.7 0.0 copy-start.2
  89.7 0.6 copy.19
  90.4 0.2 copy-done.2
  90.6 0.0 copy-start.1
  90.6 0.6 copy.20
  91.2 0.2 copy-done.1
  91.4 0.0 copy-start
  91.4 0.6 copy.21
  92.1 0.2 copy-done
  92.3 0.6 copy.22
Async XLA Ops:
  87.4 2.3 %copy-start.3 = (bf16[128,256]{1,0:T(8,128)(2,1)S(1)}, bf16[128,256]{1,0:T(8,128)(2,1)}, u32[]{:S(2)}) copy-start(bf16[128,256]{1,0:T(8,128)(2,1)} %get-tuple-element.21) | copy-start | bytes 196612
  89.7 0.9 copy-start.2
  90.6 0.9 copy-start.1
  91.4 0.9 copy-start

commit v2 on v1

v2 whole, which is shorter than its diff:
```python
import jax
import jax.numpy as jnp
from jax import lax
from jax.experimental import pallas as pl
from jax.experimental.pallas import tpu as pltpu
from jax.sharding import Mesh
from jax.sharding import PartitionSpec as P

FS = ("z", "y")
TP = ("x", "c")
MESH = pl.DeviceIdType.MESH
F32 = jnp.float32
BF16 = jnp.bfloat16
BLOCK_AXIS = ("z", "y")
SUB_AXIS = ("y", "z")


def nn(left, right):
    return lax.dot_general(left, right, (((1,), (0,)), ((), ())), preferred_element_type=F32)


def tn(left, right):
    return lax.dot_general(left, right, (((0,), (0,)), ((), ())), preferred_element_type=F32)


def square_relu(value):
    return jnp.square(jnp.maximum(value.astype(F32), 0.0)).astype(BF16)


def kernel(
    late_in_h, up_t_h, down_h, early_in_h, early_pre_h, cot_h, up_sum_h, down_sum_h,
    late_pre_o, late_out_o, input_grad_o, up_total_o, down_total_o,
    late_in, up_t, down, early_in, early_pre, cot, up_sum, down_sum, weights, grads, ring_in, last_in, early_t, cot_t, late_t, part, pair_in, pair_sum, x_in, full, acc,
    in_sem, own_sem, ag1_s, ag1_r, ag2_s, ag2_r, rs1_s, rs1_r, rs2_s, rs2_r,
    tp_s, pair_r, xr_r, xg_r, fw_r,
):
    iz, iy, ix, ic = (lax.axis_index(name) for name in ("z", "y", "x", "c"))
    place = (iz, iy)
    sub_place = (iy, iz)
    shards = (down, up_t)

    def up_by(value, step, size=8):
        return lax.rem(value + (step % size), size)

    def send(src, dst, send_sem, recv_sem, axis, index):
        pltpu.make_async_remote_copy(
            src_ref=src, dst_ref=dst, send_sem=send_sem, recv_sem=recv_sem,
            device_id={axis: index}, device_id_type=MESH,
        ).start()

    def arrive(ref, recv_sem):
        pltpu.make_async_remote_copy(
            src_ref=ref, dst_ref=ref, send_sem=recv_sem, recv_sem=recv_sem,
            device_id={"c": up_by(ic, 1, 2)}, device_id_type=MESH,
        ).wait_recv()

    def gone(ref, send_sem):
        pltpu.make_async_remote_copy(
            src_ref=ref, dst_ref=ref, send_sem=send_sem, recv_sem=send_sem,
            device_id={"c": up_by(ic, 1, 2)}, device_id_type=MESH,
        ).wait_send()

    barrier = pltpu.get_barrier_semaphore()
    for axis, me, size in (("y", iy, 8), ("z", iz, 8), ("x", ix, 4), ("c", ic, 2)):
        for step in range(1, size):
            pl.semaphore_signal(
                barrier, inc=1, device_id={axis: up_by(me, step, size)}, device_id_type=MESH
            )
    loads = []
    for at, (source, target) in enumerate((
        (down_h, down), (up_t_h, up_t), (cot_h, cot), (late_in_h, late_in), (early_pre_h, early_pre),
        (early_in_h, early_in), (down_sum_h, down_sum), (up_sum_h, up_sum),
    )):
        copy = pltpu.make_async_copy(source, target, in_sem.at[at])
        copy.start()
        loads.append(copy)
    loads[0].wait()
    pl.semaphore_wait(barrier, 18)

    own = []

    def own_copy(w):
        if w == 1:
            loads[1].wait()
        for h in range(2):
            rows = shards[w].at[pl.ds(32 * h, 32), :]
            copy = pltpu.make_async_copy(rows, weights.at[w, h, place[h], sub_place[h]], own_sem.at[w, h])
            copy.start()
            own.append(copy)

    def ag1_send(w):
        for step in (4, 3, 5, 2, 6, 1, 7):
            for h in range(2):
                rows = shards[w].at[pl.ds(32 * h, 32), :]
                target = weights.at[w, h, place[h], sub_place[h]]
                send(rows, target, ag1_s.at[w], ag1_r.at[0], SUB_AXIS[h], up_by(sub_place[h], step))

    def ag1_wait(w):
        for h in range(2):
            own[2 * w + h].wait()
        arrive(weights.at[w, 0, pl.ds(0, 7), pl.ds(0, 2)], ag1_r.at[0])

    def ring_send(w, h, way, step):
        sign = (1 - 2 * way) * (1 - 2 * h)
        ref = weights.at[w, h, place[h], up_by(sub_place[h], -sign * (step - 1))]
        send(ref, ref, ag1_s.at[w], ag1_r.at[step], SUB_AXIS[h], up_by(sub_place[h], sign))

    def ag1_ring_start(w):
        for h in range(2):
            own[2 * w + h].wait()
            for way in range(2):
                ring_send(w, h, way, 1)

    def ag1_ring_step(w, step):
        arrive(weights.at[w, 0, 0, pl.ds(0, 4 if step < 4 else 2)], ag1_r.at[step])
        for h in range(2):
            for way in range(2):
                if step + way < 4:
                    ring_send(w, h, way, step + 1)

    def ag2_send(w, h, way, step, part_at):
        sign = 1 - 2 * way
        ref = weights.at[w, h, up_by(place[h], -sign * (step - 1)), pl.ds(4 * part_at, 4)]
        send(ref, ref, ag2_s.at[w, h], ag2_r.at[w, h, step - 1, part_at], BLOCK_AXIS[h], up_by(place[h], sign))

    def ag2_start(w):
        for part_at in range(2):
            for h in range(2):
                for way in range(2):
                    ag2_send(w, h, way, 1, part_at)

    def ag2_part(w, step, part_at):
        for h in range(2):
            size = 8 if step < 4 else 4
            arrive(weights.at[w, h, 0, pl.ds(0, size)], ag2_r.at[w, h, step - 1, part_at])
            for way in range(2):
                if step < 3 or (step == 3 and part_at == way):
                    ag2_send(w, h, way, step + 1, part_at)

    def rs_send(w, h, way, step, part_at):
        sign = 1 - 2 * way
        send(
            grads.at[w, h, up_by(place[h], sign * (5 - step)), pl.ds(4 * part_at, 4)],
            ring_in.at[w, h, way, step - 1, pl.ds(4 * part_at, 4)],
            rs1_s.at[w, h], rs1_r.at[w, h, step - 1, part_at], BLOCK_AXIS[h], up_by(place[h], sign),
        )

    def rs_start(w):
        for h in range(2):
            for way in range(2):
                rs_send(w, h, way, 1, way)
        for h in range(2):
            for way in range(2):
                rs_send(w, h, way, 2, 1 - way)

    def rs_part(w, step, part_at):
        for h in range(2):
            size = 8 if step > 1 else 4
            arrive(weights.at[w, h, 0, pl.ds(0, size)], rs1_r.at[w, h, step - 1, part_at])
            for way in range(2):
                if step == 1 and part_at != way:
                    continue
                arrived = ring_in.at[w, h, way, step - 1, pl.ds(4 * part_at, 4)]
                block = up_by(place[h], (1 - 2 * way) * (4 - step))
                mine = grads.at[w, h, block, pl.ds(4 * part_at, 4)]
                mine[...] = (mine[...].astype(F32) + arrived[...].astype(F32)).astype(BF16)
                rs_send(w, h, way, step + 1, part_at)

    def rs_last(w, part_at):
        for h in range(2):
            arrive(weights.at[w, h, 0], rs1_r.at[w, h, 3, part_at])
            mine = grads.at[w, h, place[h], pl.ds(4 * part_at, 4)]
            total = mine[...].astype(F32)
            for way in range(2):
                total = total + ring_in[w, h, way, 3, pl.ds(4 * part_at, 4)].astype(F32)
            mine[...] = total.astype(BF16)

    def rs2_send(w):
        for step in (4, 3, 5, 2, 6, 1, 7):
            for h in range(2):
                send(
                    grads.at[w, h, place[h], up_by(sub_place[h], step)], last_in.at[w, h, step - 1],
                    rs2_s.at[w], rs2_r.at[0], SUB_AXIS[h], up_by(sub_place[h], step),
                )

    def rs2_ring_send(w, h, way, step):
        sign = (1 - 2 * way) * (1 - 2 * h)
        send(
            grads.at[w, h, place[h], up_by(sub_place[h], sign * (5 - way - step))],
            last_in.at[w, h, 4 * way + step - 1],
            rs2_s.at[w], rs2_r.at[step], SUB_AXIS[h], up_by(sub_place[h], sign),
        )

    def rs2_ring_start(w):
        for h in range(2):
            for way in range(2):
                rs2_ring_send(w, h, way, 1)

    def rs2_ring_step(w, step):
        arrive(weights.at[w, 0, 0, pl.ds(0, 4)], rs2_r.at[step])
        for h in range(2):
            for way in range(2):
                if step + way < 4:
                    sign = (1 - 2 * way) * (1 - 2 * h)
                    mine = grads.at[w, h, place[h], up_by(sub_place[h], sign * (4 - way - step))]
                    arrived = last_in[w, h, 4 * way + step - 1]
                    mine[...] = (mine[...].astype(F32) + arrived.astype(F32)).astype(BF16)
                    rs2_ring_send(w, h, way, step + 1)

    def rs_out(w, ring):
        base, out = ((down_sum, down_total_o), (up_sum, up_total_o))[w]
        if ring:
            arrive(weights.at[w, 0, 0, pl.ds(0, 2)], rs2_r.at[4])
        else:
            arrive(weights.at[w, 0, pl.ds(0, 7), pl.ds(0, 2)], rs2_r.at[0])
        for h in range(2):
            total = grads[w, h, place[h], sub_place[h]].astype(F32)
            for at in (3, 6) if ring else range(7):
                total = total + last_in[w, h, at].astype(F32)
            rows = pl.ds(32 * h, 32)
            out[rows, :] = base[rows, :] + total

    def block_of(h, side, j):
        return lax.rem(iz * (1 - h) + iy * h + side * (2 * j + 1) - j + 8, 8)

    def product(a, j, sides):
        w, right = ((0, cot_t), (1, late_t))[a]

        def one(h, _):
            for side in sides:
                rows = weights[w, h, block_of(h, side, j)].reshape(256, 256)
                part[a, j, pl.ds(pl.multiple_of(h * 512 + side * 256, 256), 256), :] = nn(
                    rows, right[...]
                ).astype(BF16)
            return 0

        lax.fori_loop(0, 2, one, 0)

    other = up_by(ic, 1, 2)
    my_half = pl.multiple_of(ic * 512, 512)
    other_half = pl.multiple_of(other * 512, 512)

    def s1(a, j):
        send(
            part.at[a, j, pl.ds(other_half, 512), :], pair_in.at[a, j],
            tp_s.at[a, 0], pair_r.at[a, j], "c", other,
        )

    def s2(a, j):
        arrive(pair_in.at[a, j], pair_r.at[a, j])
        pair_sum[a, j] = (
            part[a, j, pl.ds(my_half, 512), :].astype(F32) + pair_in[a, j].astype(F32)
        ).astype(BF16)
        for step in (2, 1, 3):
            target = up_by(ix, step, 4)
            rows = pl.ds(pl.multiple_of(target * 128, 128), 128)
            send(pair_sum.at[a, j, rows, :], x_in.at[a, j, step - 1], tp_s.at[a, 1], xr_r.at[a, j], "x", target)

    def share(a, core, x, j):
        return full.at[a, core, block_of(core, x // 2, j), pl.ds(4 * lax.rem(x, 2), 4)]

    def s3(a, j):
        total = pair_sum[a, j, pl.ds(pl.multiple_of(ix * 128, 128), 128), :].astype(F32)
        arrive(x_in.at[a, j], xr_r.at[a, j])
        for at in range(3):
            total = total + x_in[a, j, at].astype(F32)
        if a == 0:
            block = block_of(ic, ix // 2, j)
            saved = early_t[ic, block, pl.ds(4 * lax.rem(ix, 2), 4)].reshape(128, 128)
            total = total * 2.0 * jnp.maximum(saved.astype(F32), 0.0)
        ref = share(a, ic, ix, j)
        ref[...] = total.astype(BF16).reshape(4, 32, 128)
        for step in (2, 1, 3):
            send(ref, ref, tp_s.at[a, 2], xg_r.at[a, j], "x", up_by(ix, step, 4))
        send(ref, ref, tp_s.at[a, 3], fw_r.at[a, j], "c", other)

    def s4(a, j):
        arrive(x_in.at[a, j], xg_r.at[a, j])
        for step in (1, 2, 3):
            ref = share(a, ic, up_by(ix, step, 4), j)
            send(ref, ref, tp_s.at[a, 3], fw_r.at[a, j], "c", other)

    def s5(a, j):
        arrive(pair_in.at[a, j], fw_r.at[a, j])

    def all_gone():
        small = weights.at[0, 0, pl.ds(0, 7), pl.ds(0, 2)]
        for w in range(2):
            gone(small, ag1_s.at[w])
            gone(small, rs2_s.at[w])
            for h in range(2):
                gone(weights.at[w, h, pl.ds(0, 7)], ag2_s.at[w, h])
                gone(weights.at[w, h, pl.ds(0, 7)], rs1_s.at[w, h])
            gone(pair_in.at[w], tp_s.at[w, 0])
            gone(x_in.at[w], tp_s.at[w, 1])
            gone(x_in.at[w], tp_s.at[w, 2])
            gone(pair_in.at[w], tp_s.at[w, 3])

    def pieces(j, fn):
        def one(at, _):
            h, side = at // 2, lax.rem(at, 2)
            fn(h, block_of(h, side, j))
            return 0

        lax.fori_loop(0, 4, one, 0)

    def up_grads(j):
        def fn(h, block):
            rows = full[0, h, block].reshape(256, 128)
            grads[1, h, block] = nn(rows, early_in[...]).astype(BF16).reshape(8, 32, 256)

        pieces(j, fn)

    def input_grads(j):
        def fn(h, block):
            acc[0] += tn(full[0, h, block].reshape(256, 128), weights[1, h, block].reshape(256, 256))

        pieces(j, fn)

    def late_outs(j):
        def fn(h, block):
            hidden = square_relu(full[1, h, block].reshape(256, 128))
            acc[1] += tn(hidden, weights[0, h, block].reshape(256, 256))

        pieces(j, fn)

    def early(quarter):
        def one(at, _):
            z, y = at // 4, 2 * lax.rem(at, 4)
            turned = early_pre[:, pl.ds(pl.multiple_of(at * 128, 128), 128)].T
            early_t[0, z, y] = turned[0:32]
            early_t[1, y, z] = turned[32:64]
            early_t[0, z, y + 1] = turned[64:96]
            early_t[1, y + 1, z] = turned[96:128]
            return 0

        if quarter == 0:
            loads[4].wait()
        lax.fori_loop(8 * quarter, 8 * quarter + 8, one, 0)

    def turn_late(quarter):
        def one(at, _):
            z, y = at // 4, 2 * lax.rem(at, 4)
            rows = jnp.concatenate(
                [full[1, 0, z, y], full[1, 1, y, z], full[1, 0, z, y + 1], full[1, 1, y + 1, z]], axis=0
            )
            late_pre_o[:, pl.ds(pl.multiple_of(at * 128, 128), 128)] = rows.T
            return 0

        lax.fori_loop(8 * quarter, 8 * quarter + 8, one, 0)

    def down_grads(j):
        def fn(h, block):
            hidden = square_relu(early_t[h, block].reshape(256, 128))
            grads[0, h, block] = nn(hidden, cot[...]).astype(BF16).reshape(8, 32, 256)

        pieces(j, fn)

    def prep_cot():
        loads[2].wait()
        cot_t[...] = cot[...].T

    def prep_late():
        loads[3].wait()
        late_t[...] = late_in[...].T
        acc[...] = jnp.zeros_like(acc)
        loads[5].wait()
        loads[6].wait()
        loads[7].wait()

    def fin_late():
        late_out_o[...] = acc[1].astype(BF16)

    def fin_input():
        input_grad_o[...] = acc[0].astype(BF16)

    own_copy(0)
    ag1_send(0)
    own_copy(1)
    early(0)
    early(1)
    early(2)
    early(3)
    prep_cot()
    down_grads(1)
    down_grads(3)
    down_grads(0)
    ag1_wait(0)
    ag2_start(0)
    product(0, 0, (0,))
    ag1_ring_start(1)
    prep_late()
    down_grads(2)
    rs_start(0)
    ag2_part(0, 1, 0)
    ag2_part(0, 1, 1)
    product(0, 0, (1,))
    s1(0, 0)
    ag1_ring_step(1, 1)
    product(0, 1, (0,))
    rs_part(0, 1, 1)
    rs_part(0, 1, 0)
    s2(0, 0)
    ag2_part(0, 2, 0)
    ag2_part(0, 2, 1)
    product(0, 1, (1,))
    ag1_ring_step(1, 2)
    s1(0, 1)
    product(0, 2, (0,))
    s3(0, 0)
    s2(0, 1)
    rs_part(0, 2, 0)
    rs_part(0, 2, 1)
    ag2_part(0, 3, 0)
    ag2_part(0, 3, 1)
    product(0, 3, (0,))
    ag1_ring_step(1, 3)
    product(0, 2, (1,))
    s1(0, 2)
    s4(0, 0)
    rs_part(0, 3, 0)
    s2(0, 2)
    s5(0, 0)
    up_grads(0)
    s3(0, 1)
    rs_part(0, 3, 1)
    ag2_part(0, 4, 0)
    ag2_part(0, 4, 1)
    product(0, 3, (1,))
    s1(0, 3)
    ag1_ring_step(1, 4)
    ag2_start(1)
    product(1, 0, (0,))
    s2(0, 3)
    rs_last(0, 0)
    s3(0, 2)
    rs_last(0, 1)
    rs2_ring_start(0)
    s4(0, 1)
    ag2_part(1, 1, 0)
    s5(0, 1)
    up_grads(1)
    ag2_part(1, 1, 1)
    product(1, 1, (0,))
    s3(0, 3)
    rs2_ring_step(0, 1)
    product(1, 0, (1,))
    s1(1, 0)
    s4(0, 2)
    ag2_part(1, 2, 0)
    s2(1, 0)
    s5(0, 2)
    up_grads(2)
    rs2_ring_step(0, 2)
    ag2_part(1, 2, 1)
    product(1, 2, (0,))
    product(1, 1, (1,))
    s4(0, 3)
    s1(1, 1)
    ag2_part(1, 3, 0)
    s5(0, 3)
    up_grads(3)
    rs_start(1)
    rs2_ring_step(0, 3)
    s2(1, 1)
    s3(1, 0)
    ag2_part(1, 3, 1)
    product(1, 2, (1,))
    s1(1, 2)
    product(1, 3, (0,))
    ag2_part(1, 4, 0)
    s2(1, 2)
    rs_part(1, 1, 1)
    rs_part(1, 1, 0)
    s3(1, 1)
    rs_out(0, True)
    ag2_part(1, 4, 1)
    product(1, 3, (1,))
    s1(1, 3)
    input_grads(2)
    input_grads(3)
    rs_part(1, 2, 0)
    s2(1, 3)
    rs_part(1, 2, 1)
    s4(1, 0)
    input_grads(0)
    s3(1, 2)
    input_grads(1)
    s5(1, 0)
    late_outs(0)
    s4(1, 1)
    fin_input()
    rs_part(1, 3, 0)
    s5(1, 1)
    late_outs(1)
    s3(1, 3)
    rs_part(1, 3, 1)
    s4(1, 2)
    rs_last(1, 0)
    s5(1, 2)
    late_outs(2)
    rs_last(1, 1)
    rs2_send(1)
    s4(1, 3)
    s5(1, 3)
    turn_late(2)
    late_outs(3)
    turn_late(1)
    fin_late()
    turn_late(3)
    turn_late(0)
    rs_out(1, False)
    all_gone()


def deliver(*refs):
    sources, targets, sems = refs[:5], refs[5:10], refs[10]
    copies = [pltpu.make_async_copy(a, b, sems.at[at]) for at, (a, b) in enumerate(zip(sources, targets))]
    for copy in copies:
        copy.start()
    for copy in copies:
        copy.wait()


def body(late_input, up_weight, down_weight, early_input, early_pre, cotangent, up_sum, down_sum):
    vmem = pl.BlockSpec(memory_space=pltpu.VMEM)
    anywhere = pl.BlockSpec(memory_space=pl.ANY)
    dma = pltpu.SemaphoreType.DMA
    results = (((128, 4096), BF16), ((128, 256), BF16), ((128, 256), BF16), ((64, 256), F32), ((64, 256), F32))
    held = pl.pallas_call(
        kernel,
        out_shape=tuple(pltpu.VMEM(shape, dtype) for shape, dtype in results),
        in_specs=[anywhere] * 8,
        out_specs=(vmem,) * 5,
        scratch_shapes=[
            pltpu.VMEM((128, 256), BF16),
            pltpu.VMEM((64, 256), BF16),
            pltpu.VMEM((64, 256), BF16),
            pltpu.VMEM((128, 256), BF16),
            pltpu.VMEM((128, 4096), BF16),
            pltpu.VMEM((128, 256), BF16),
            pltpu.VMEM((64, 256), F32),
            pltpu.VMEM((64, 256), F32),
            pltpu.VMEM((2, 2, 8, 8, 32, 256), BF16),
            pltpu.VMEM((2, 2, 8, 8, 32, 256), BF16),
            pltpu.VMEM((2, 2, 2, 4, 8, 32, 256), BF16),
            pltpu.VMEM((2, 2, 7, 32, 256), BF16),
            pltpu.VMEM((2, 8, 8, 32, 128), BF16),
            pltpu.VMEM((256, 128), BF16),
            pltpu.VMEM((256, 128), BF16),
            pltpu.VMEM((2, 4, 1024, 128), BF16),
            pltpu.VMEM((2, 4, 512, 128), BF16),
            pltpu.VMEM((2, 4, 512, 128), BF16),
            pltpu.VMEM((2, 4, 3, 128, 128), BF16),
            pltpu.VMEM((2, 2, 8, 8, 32, 128), BF16),
            pltpu.VMEM((2, 128, 256), F32),
            dma((8,)), dma((2, 2)),
            dma((2,)), dma((5,)),
            dma((2, 2)), dma((2, 2, 4, 2)),
            dma((2, 2)), dma((2, 2, 4, 2)),
            dma((2,)), dma((5,)),
            dma((2, 4)), dma((2, 4)), dma((2, 4)), dma((2, 4)), dma((2, 4)),
        ],
        compiler_params=pltpu.CompilerParams(
            collective_id=0, has_side_effects=True, vmem_limit_bytes=36 * 1024 * 1024
        ),
        cost_estimate=pl.CostEstimate(flops=1_700_000_000, bytes_accessed=8_000_000, transcendentals=0),
    )(*(
        pltpu.with_memory_space_constraint(value, pltpu.MemorySpace.HBM)
        for value in (
            late_input, up_weight.T, down_weight, early_input, early_pre, cotangent, up_sum.T, down_sum
        )
    ))
    outs = pl.pallas_call(
        deliver,
        out_shape=tuple(jax.ShapeDtypeStruct(shape, dtype) for shape, dtype in results),
        in_specs=[vmem] * 5,
        out_specs=(anywhere,) * 5,
        scratch_shapes=[dma((5,))],
        compiler_params=pltpu.CompilerParams(vmem_limit_bytes=8 * 1024 * 1024),
    )(*held)
    late_pre, late_out, input_grad, up_total, down_total = outs
    return late_pre, late_out, input_grad, up_total.T, down_total


def solution(mesh):
    split = Mesh(mesh.devices.reshape(8, 8, 4, 2), FS + TP)
    placed = (
        P(FS, TP), P(TP, FS), P(FS, TP), P(FS, TP), P(FS, None), P(FS, TP), P(TP, FS), P(FS, TP),
    )
    return jax.shard_map(
        body,
        mesh=split,
        in_specs=placed,
        out_specs=(P(FS, None), P(FS, TP), P(FS, TP), P(TP, FS), P(FS, TP)),
        check_vma=False,
    )
```

time: 93.2 us -> 81.6 us (0.88)
  Pallas kernels: 86.7 us -> 80.8 us
  local copies, waits for them, and re-layouts: 5.54 us -> 0 us
    pallas_call x1 -> x2, Pallas kernels: 86.7 us -> 80.8 us  [the longest x1 79.7 us: body(): pl.pallas_call(kernel, out_shape=tuple((pltpu.VMEM(shape, dtype) for shap...]
    unnamed x13 -> x0, local copies, waits for them, and re-layouts: 5.54 us -> none
where the time goes in v2:
time: 81.6 us; the launch traced here: 81.5 us
  Pallas kernels  80.8 us (99%)
    pallas_call x1, Pallas kernels, body(): pl.pallas_call(kernel, out_shape=tuple((pltpu.VMEM(shape, dtype) for shap...  79.7 us

profile of v2, /device:TPU:1, one launch (start us, length us, event | category | flops | bytes accessed | tf_op | source)
XLA Modules:
  0.0 81.5 jit_solution(9931110325824607220)
XLA Ops:
  0.6 79.7 %shard_map.119 = (bf16[128,4096]{1,0:T(8,128)(2,1)S(1)}, bf16[128,256]{1,0:T(8,128)(2,1)S(1)}, bf16[128,256]{1,0:T(8,128)(2,1)S(1)}, f32[64,256]{1,0:T(8,128)S(1)}, f32[64,256]{1,0:T(8,128)S(1)}) custom-call(bf16[128,256]{1,0:T(8,128)(2,1)} %late_in_h.1, bf16[64,256]{1,0:T(8,128)(2,1)} %bitcast.5, bf16[64,256]{1,0:T(8,128)(2,1)} %down_h.1, ...), custom_call_target="tpu_custom_call" | custom-call | flops 1700000000 | bytes 8000000 | tf_op jit(solution)/shard_map/pallas_call | solution.py:530
  80.4 1.1 %shard_map.120 = (bf16[128,4096]{1,0:T(8,128)(2,1)}, bf16[128,256]{1,0:T(8,128)(2,1)}, bf16[128,256]{1,0:T(8,128)(2,1)}, f32[64,256]{1,0:T(8,128)}, f32[64,256]{1,0:T(8,128)}) custom-call(bf16[128,4096]{1,0:T(8,128)(2,1)S(1)} %get-tuple-element.15.refs_0_, bf16[128,256]{1,0:T(8,128)(2,1)S(1)} %get-tuple-element.16.refs_1_, ...), custom_call_target="tpu_custom_call" | custom-call | tf_op jit(solution)/shard_map/pallas_call | solution.py:574

commit v3 on v2

--- a/solution.py
+++ b/solution.py
@@ -13,6 +13,8 @@
 BF16 = jnp.bfloat16
 BLOCK_AXIS = ("z", "y")
 SUB_AXIS = ("y", "z")
+GATHER_PARTS = (4, 4)
+SCATTER_PARTS = (4, 4)
 
 
 def nn(left, right):
@@ -30,7 +32,8 @@
 def kernel(
     late_in_h, up_t_h, down_h, early_in_h, early_pre_h, cot_h, up_sum_h, down_sum_h,
     late_pre_o, late_out_o, input_grad_o, up_total_o, down_total_o,
-    late_in, up_t, down, early_in, early_pre, cot, up_sum, down_sum, weights, grads, ring_in, last_in, early_t, cot_t, late_t, part, pair_in, pair_sum, x_in, full, acc,
+    late_in, up_t, down, early_in, early_pre, cot, up_sum, down_sum,
+    weights, grads, ring_in, last_in, early_t, cot_t, late_t, part, pair_in, pair_sum, x_in, full, acc,
     in_sem, own_sem, ag1_s, ag1_r, ag2_s, ag2_r, rs1_s, rs1_r, rs2_s, rs2_r,
     tp_s, pair_r, xr_r, xg_r, fw_r,
 ):
@@ -74,6 +77,27 @@
         copy = pltpu.make_async_copy(source, target, in_sem.at[at])
         copy.start()
         loads.append(copy)
+    def slot(sub, h):
+        return lax.rem(sub - sub_place[h] + 9, 8)
+
+    def early(quarter):
+        def one(at, _):
+            z, y = at // 4, 2 * lax.rem(at, 4)
+            turned = early_pre[:, pl.ds(pl.multiple_of(at * 128, 128), 128)].T
+            early_t[0, z, slot(y, 0)] = turned[0:32]
+            early_t[1, y, slot(z, 1)] = turned[32:64]
+            early_t[0, z, slot(y + 1, 0)] = turned[64:96]
+            early_t[1, y + 1, slot(z, 1)] = turned[96:128]
+            return 0
+
+        lax.fori_loop(8 * quarter, 8 * quarter + 8, one, 0)
+
+    loads[2].wait()
+    cot_t[...] = cot[...].T
+    loads[4].wait()
+    early(0)
+    early(1)
+    early(2)
     loads[0].wait()
     pl.semaphore_wait(barrier, 18)
 
@@ -84,26 +108,35 @@
             loads[1].wait()
         for h in range(2):
             rows = shards[w].at[pl.ds(32 * h, 32), :]
-            copy = pltpu.make_async_copy(rows, weights.at[w, h, place[h], sub_place[h]], own_sem.at[w, h])
+            copy = pltpu.make_async_copy(rows, weights.at[w, h, place[h], 1], own_sem.at[w, h])
             copy.start()
             own.append(copy)
 
+    def others_in(part_at, parts):
+        slots = range(part_at * 8 // parts, (part_at + 1) * 8 // parts)
+        return [at for at in slots if at != 1]
+
     def ag1_send(w):
-        for step in (4, 3, 5, 2, 6, 1, 7):
+        for part_at in range(GATHER_PARTS[w]):
+            for at in others_in(part_at, GATHER_PARTS[w])[::-1]:
+                for h in range(2):
+                    send(
+                        shards[w].at[pl.ds(32 * h, 32), :], weights.at[w, h, place[h], at],
+                        ag1_s.at[w], ag1_r.at[5 + part_at], SUB_AXIS[h], up_by(sub_place[h], 1 - at),
+                    )
+
+    def ag1_wait(w, part_at):
+        if part_at == 0:
             for h in range(2):
-                rows = shards[w].at[pl.ds(32 * h, 32), :]
-                target = weights.at[w, h, place[h], sub_place[h]]
-                send(rows, target, ag1_s.at[w], ag1_r.at[0], SUB_AXIS[h], up_by(sub_place[h], step))
-
-    def ag1_wait(w):
-        for h in range(2):
-            own[2 * w + h].wait()
-        arrive(weights.at[w, 0, pl.ds(0, 7), pl.ds(0, 2)], ag1_r.at[0])
+                own[2 * w + h].wait()
+        count = len(others_in(part_at, GATHER_PARTS[w]))
+        arrive(weights.at[w, 0, pl.ds(0, 2), pl.ds(0, count)], ag1_r.at[5 + part_at])
 
     def ring_send(w, h, way, step):
         sign = (1 - 2 * way) * (1 - 2 * h)
-        ref = weights.at[w, h, place[h], up_by(sub_place[h], -sign * (step - 1))]
-        send(ref, ref, ag1_s.at[w], ag1_r.at[step], SUB_AXIS[h], up_by(sub_place[h], sign))
+        ref = weights.at[w, h, place[h], (9 - sign * (step - 1)) % 8]
+        target = weights.at[w, h, place[h], (9 - sign * step) % 8]
+        send(ref, target, ag1_s.at[w], ag1_r.at[step], SUB_AXIS[h], up_by(sub_place[h], sign))
 
     def ag1_ring_start(w):
         for h in range(2):
@@ -120,73 +153,77 @@
 
     def ag2_send(w, h, way, step, part_at):
         sign = 1 - 2 * way
-        ref = weights.at[w, h, up_by(place[h], -sign * (step - 1)), pl.ds(4 * part_at, 4)]
+        size = 8 // GATHER_PARTS[w]
+        ref = weights.at[w, h, up_by(place[h], -sign * (step - 1)), pl.ds(size * part_at, size)]
         send(ref, ref, ag2_s.at[w, h], ag2_r.at[w, h, step - 1, part_at], BLOCK_AXIS[h], up_by(place[h], sign))
 
-    def ag2_start(w):
-        for part_at in range(2):
-            for h in range(2):
-                for way in range(2):
-                    ag2_send(w, h, way, 1, part_at)
+    def ag2_start(w, part_at):
+        for h in range(2):
+            for way in range(2):
+                ag2_send(w, h, way, 1, part_at)
 
     def ag2_part(w, step, part_at):
-        for h in range(2):
-            size = 8 if step < 4 else 4
+        parts = GATHER_PARTS[w]
+        size = (16 if step < 4 else 8) // parts
+        for h in range(2):
             arrive(weights.at[w, h, 0, pl.ds(0, size)], ag2_r.at[w, h, step - 1, part_at])
             for way in range(2):
-                if step < 3 or (step == 3 and part_at == way):
+                if step < 3 or (step == 3 and 2 * part_at // parts == way):
                     ag2_send(w, h, way, step + 1, part_at)
 
     def rs_send(w, h, way, step, part_at):
         sign = 1 - 2 * way
+        size = 8 // SCATTER_PARTS[w]
         send(
-            grads.at[w, h, up_by(place[h], sign * (5 - step)), pl.ds(4 * part_at, 4)],
-            ring_in.at[w, h, way, step - 1, pl.ds(4 * part_at, 4)],
+            grads.at[w, h, up_by(place[h], sign * (5 - step)), pl.ds(size * part_at, size)],
+            ring_in.at[w, h, way, step - 1, pl.ds(size * part_at, size)],
             rs1_s.at[w, h], rs1_r.at[w, h, step - 1, part_at], BLOCK_AXIS[h], up_by(place[h], sign),
         )
 
     def rs_start(w):
-        for h in range(2):
-            for way in range(2):
-                rs_send(w, h, way, 1, way)
-        for h in range(2):
-            for way in range(2):
-                rs_send(w, h, way, 2, 1 - way)
+        parts = SCATTER_PARTS[w]
+        for step in (1, 2):
+            for part_at in ((1, 0), (2, 3, 1, 0))[parts // 4]:
+                way = (2 * part_at // parts + step - 1) % 2
+                for h in range(2):
+                    rs_send(w, h, way, step, part_at)
 
     def rs_part(w, step, part_at):
-        for h in range(2):
-            size = 8 if step > 1 else 4
-            arrive(weights.at[w, h, 0, pl.ds(0, size)], rs1_r.at[w, h, step - 1, part_at])
-            for way in range(2):
-                if step == 1 and part_at != way:
+        parts = SCATTER_PARTS[w]
+        size = 8 // parts
+        for h in range(2):
+            arrive(weights.at[w, h, 0, pl.ds(0, 2 * size if step > 1 else size)], rs1_r.at[w, h, step - 1, part_at])
+            for way in range(2):
+                if step == 1 and 2 * part_at // parts != way:
                     continue
-                arrived = ring_in.at[w, h, way, step - 1, pl.ds(4 * part_at, 4)]
+                arrived = ring_in.at[w, h, way, step - 1, pl.ds(size * part_at, size)]
                 block = up_by(place[h], (1 - 2 * way) * (4 - step))
-                mine = grads.at[w, h, block, pl.ds(4 * part_at, 4)]
+                mine = grads.at[w, h, block, pl.ds(size * part_at, size)]
                 mine[...] = (mine[...].astype(F32) + arrived[...].astype(F32)).astype(BF16)
                 rs_send(w, h, way, step + 1, part_at)
 
     def rs_last(w, part_at):
-        for h in range(2):
-            arrive(weights.at[w, h, 0], rs1_r.at[w, h, 3, part_at])
-            mine = grads.at[w, h, place[h], pl.ds(4 * part_at, 4)]
+        size = 8 // SCATTER_PARTS[w]
+        for h in range(2):
+            arrive(weights.at[w, h, 0, pl.ds(0, 2 * size)], rs1_r.at[w, h, 3, part_at])
+            mine = grads.at[w, h, place[h], pl.ds(size * part_at, size)]
             total = mine[...].astype(F32)
             for way in range(2):
-                total = total + ring_in[w, h, way, 3, pl.ds(4 * part_at, 4)].astype(F32)
+                total = total + ring_in[w, h, way, 3, pl.ds(size * part_at, size)].astype(F32)
             mine[...] = total.astype(BF16)
 
-    def rs2_send(w):
-        for step in (4, 3, 5, 2, 6, 1, 7):
+    def rs2_send(w, part_at):
+        for at in others_in(part_at, SCATTER_PARTS[w])[::-1]:
             for h in range(2):
                 send(
-                    grads.at[w, h, place[h], up_by(sub_place[h], step)], last_in.at[w, h, step - 1],
-                    rs2_s.at[w], rs2_r.at[0], SUB_AXIS[h], up_by(sub_place[h], step),
+                    grads.at[w, h, place[h], at], last_in.at[w, h, (at - 2) % 8],
+                    rs2_s.at[w], rs2_r.at[5 + part_at], SUB_AXIS[h], up_by(sub_place[h], at - 1),
                 )
 
     def rs2_ring_send(w, h, way, step):
         sign = (1 - 2 * way) * (1 - 2 * h)
         send(
-            grads.at[w, h, place[h], up_by(sub_place[h], sign * (5 - way - step))],
+            grads.at[w, h, place[h], (sign * (5 - way - step) + 1) % 8],
             last_in.at[w, h, 4 * way + step - 1],
             rs2_s.at[w], rs2_r.at[step], SUB_AXIS[h], up_by(sub_place[h], sign),
         )
@@ -202,7 +239,7 @@
             for way in range(2):
                 if step + way < 4:
                     sign = (1 - 2 * way) * (1 - 2 * h)
-                    mine = grads.at[w, h, place[h], up_by(sub_place[h], sign * (4 - way - step))]
+                    mine = grads.at[w, h, place[h], (sign * (4 - way - step) + 1) % 8]
                     arrived = last_in[w, h, 4 * way + step - 1]
                     mine[...] = (mine[...].astype(F32) + arrived.astype(F32)).astype(BF16)
                     rs2_ring_send(w, h, way, step + 1)
@@ -212,9 +249,11 @@
         if ring:
             arrive(weights.at[w, 0, 0, pl.ds(0, 2)], rs2_r.at[4])
         else:
-            arrive(weights.at[w, 0, pl.ds(0, 7), pl.ds(0, 2)], rs2_r.at[0])
-        for h in range(2):
-            total = grads[w, h, place[h], sub_place[h]].astype(F32)
+            for part_at in range(SCATTER_PARTS[w]):
+                count = len(others_in(part_at, SCATTER_PARTS[w]))
+                arrive(weights.at[w, 0, pl.ds(0, 2), pl.ds(0, count)], rs2_r.at[5 + part_at])
+        for h in range(2):
+            total = grads[w, h, place[h], 1].astype(F32)
             for at in (3, 6) if ring else range(7):
                 total = total + last_in[w, h, at].astype(F32)
             rows = pl.ds(32 * h, 32)
@@ -324,25 +363,15 @@
 
         pieces(j, fn)
 
-    def early(quarter):
-        def one(at, _):
-            z, y = at // 4, 2 * lax.rem(at, 4)
-            turned = early_pre[:, pl.ds(pl.multiple_of(at * 128, 128), 128)].T
-            early_t[0, z, y] = turned[0:32]
-            early_t[1, y, z] = turned[32:64]
-            early_t[0, z, y + 1] = turned[64:96]
-            early_t[1, y + 1, z] = turned[96:128]
-            return 0
-
-        if quarter == 0:
-            loads[4].wait()
-        lax.fori_loop(8 * quarter, 8 * quarter + 8, one, 0)
-
     def turn_late(quarter):
         def one(at, _):
             z, y = at // 4, 2 * lax.rem(at, 4)
             rows = jnp.concatenate(
-                [full[1, 0, z, y], full[1, 1, y, z], full[1, 0, z, y + 1], full[1, 1, y + 1, z]], axis=0
+                [
+                    full[1, 0, z, slot(y, 0)], full[1, 1, y, slot(z, 1)],
+                    full[1, 0, z, slot(y + 1, 0)], full[1, 1, y + 1, slot(z, 1)],
+                ],
+                axis=0,
             )
             late_pre_o[:, pl.ds(pl.multiple_of(at * 128, 128), 128)] = rows.T
             return 0
@@ -355,10 +384,6 @@
             grads[0, h, block] = nn(hidden, cot[...]).astype(BF16).reshape(8, 32, 256)
 
         pieces(j, fn)
-
-    def prep_cot():
-        loads[2].wait()
-        cot_t[...] = cot[...].T
 
     def prep_late():
         loads[3].wait()
@@ -376,139 +401,179 @@
 
     own_copy(0)
     ag1_send(0)
+    early(3)
+    down_grads(2)
+    down_grads(0)
     own_copy(1)
-    early(0)
-    early(1)
-    early(2)
-    early(3)
-    prep_cot()
+    prep_late()
     down_grads(1)
     down_grads(3)
-    down_grads(0)
-    ag1_wait(0)
-    ag2_start(0)
+    ag1_wait(0, 0)
+    ag1_wait(0, 1)
+    ag2_start(0, 0)
+    ag2_start(0, 1)
+    ag1_ring_start(1)
+    ag1_wait(0, 2)
+    ag2_start(0, 2)
+    ag1_wait(0, 3)
+    ag2_start(0, 3)
     product(0, 0, (0,))
-    ag1_ring_start(1)
-    prep_late()
-    down_grads(2)
-    rs_start(0)
     ag2_part(0, 1, 0)
+    ag1_ring_step(1, 1)
+    ag2_start(1, 0)
+    ag2_part(0, 1, 2)
     ag2_part(0, 1, 1)
+    ag2_part(0, 1, 3)
     product(0, 0, (1,))
+    product(0, 1, (0,))
+    ag2_part(0, 2, 0)
     s1(0, 0)
-    ag1_ring_step(1, 1)
-    product(0, 1, (0,))
-    rs_part(0, 1, 1)
-    rs_part(0, 1, 0)
+    ag1_ring_step(1, 2)
+    ag2_start(1, 1)
+    ag2_part(1, 1, 0)
     s2(0, 0)
-    ag2_part(0, 2, 0)
+    ag2_part(0, 2, 2)
     ag2_part(0, 2, 1)
+    ag2_part(0, 2, 3)
     product(0, 1, (1,))
-    ag1_ring_step(1, 2)
     s1(0, 1)
     product(0, 2, (0,))
+    ag2_part(0, 3, 0)
+    ag1_ring_step(1, 3)
+    s2(0, 1)
+    ag2_part(1, 2, 0)
+    ag2_start(1, 3)
     s3(0, 0)
-    s2(0, 1)
-    rs_part(0, 2, 0)
-    rs_part(0, 2, 1)
-    ag2_part(0, 3, 0)
+    ag2_part(0, 3, 2)
     ag2_part(0, 3, 1)
-    product(0, 3, (0,))
-    ag1_ring_step(1, 3)
+    ag2_part(0, 3, 3)
     product(0, 2, (1,))
     s1(0, 2)
+    ag2_part(1, 1, 1)
+    product(0, 3, (0,))
+    ag2_part(0, 4, 0)
+    ag1_ring_step(1, 4)
+    ag2_start(1, 2)
+    product(1, 0, (0,))
+    ag2_part(1, 3, 0)
+    s2(0, 2)
+    s3(0, 1)
+    ag2_part(1, 1, 3)
+    ag2_part(0, 4, 2)
+    ag2_part(0, 4, 1)
+    rs_start(0)
+    ag2_part(0, 4, 3)
+    product(0, 3, (1,))
+    s1(0, 3)
+    ag2_part(1, 2, 1)
     s4(0, 0)
-    rs_part(0, 3, 0)
-    s2(0, 2)
+    ag2_part(1, 1, 2)
+    product(1, 0, (1,))
+    s1(1, 0)
+    s2(0, 3)
+    product(1, 1, (0,))
+    ag2_part(1, 4, 0)
     s5(0, 0)
     up_grads(0)
-    s3(0, 1)
-    rs_part(0, 3, 1)
-    ag2_part(0, 4, 0)
-    ag2_part(0, 4, 1)
-    product(0, 3, (1,))
-    s1(0, 3)
-    ag1_ring_step(1, 4)
-    ag2_start(1)
-    product(1, 0, (0,))
-    s2(0, 3)
-    rs_last(0, 0)
+    ag2_part(1, 2, 3)
     s3(0, 2)
-    rs_last(0, 1)
-    rs2_ring_start(0)
+    rs_part(0, 1, 2)
+    rs_part(0, 1, 0)
+    rs_part(0, 1, 3)
+    rs_part(0, 1, 1)
     s4(0, 1)
-    ag2_part(1, 1, 0)
+    ag2_part(1, 3, 1)
     s5(0, 1)
     up_grads(1)
-    ag2_part(1, 1, 1)
-    product(1, 1, (0,))
+    ag2_part(1, 2, 2)
     s3(0, 3)
-    rs2_ring_step(0, 1)
-    product(1, 0, (1,))
-    s1(1, 0)
+    product(1, 1, (1,))
+    ag2_part(1, 3, 3)
+    s1(1, 1)
+    product(1, 2, (0,))
+    rs_part(0, 2, 2)
+    rs_part(0, 2, 3)
+    rs_part(0, 2, 1)
+    s2(1, 1)
     s4(0, 2)
-    ag2_part(1, 2, 0)
-    s2(1, 0)
+    ag2_part(1, 4, 1)
+    rs_part(0, 2, 0)
+    ag2_part(1, 3, 2)
+    product(1, 2, (1,))
+    product(1, 3, (0,))
     s5(0, 2)
     up_grads(2)
-    rs2_ring_step(0, 2)
-    ag2_part(1, 2, 1)
-    product(1, 2, (0,))
-    product(1, 1, (1,))
+    rs_part(0, 3, 2)
+    s1(1, 2)
+    ag2_part(1, 4, 3)
+    s2(1, 0)
     s4(0, 3)
-    s1(1, 1)
-    ag2_part(1, 3, 0)
+    rs_part(0, 3, 3)
+    s2(1, 2)
+    rs_part(0, 3, 1)
     s5(0, 3)
     up_grads(3)
     rs_start(1)
-    rs2_ring_step(0, 3)
-    s2(1, 1)
+    rs_part(0, 3, 0)
+    s3(1, 1)
+    ag2_part(1, 4, 2)
+    product(1, 3, (1,))
+    input_grads(3)
+    s1(1, 3)
+    input_grads(0)
+    rs_last(0, 2)
+    input_grads(2)
+    rs_last(0, 1)
+    rs_part(1, 1, 2)
+    s2(1, 3)
+    rs_last(0, 3)
+    input_grads(1)
+    fin_input()
+    rs_part(1, 1, 3)
+    rs_part(1, 1, 0)
     s3(1, 0)
-    ag2_part(1, 3, 1)
-    product(1, 2, (1,))
-    s1(1, 2)
-    product(1, 3, (0,))
-    ag2_part(1, 4, 0)
-    s2(1, 2)
+    s3(1, 2)
     rs_part(1, 1, 1)
-    rs_part(1, 1, 0)
-    s3(1, 1)
-    rs_out(0, True)
-    ag2_part(1, 4, 1)
-    product(1, 3, (1,))
-    s1(1, 3)
-    input_grads(2)
-    input_grads(3)
+    rs_last(0, 0)
+    rs2_ring_start(0)
+    rs_part(1, 2, 2)
+    s4(1, 1)
+    rs_part(1, 2, 3)
     rs_part(1, 2, 0)
-    s2(1, 3)
     rs_part(1, 2, 1)
-    s4(1, 0)
-    input_grads(0)
-    s3(1, 2)
-    input_grads(1)
-    s5(1, 0)
-    late_outs(0)
-    s4(1, 1)
-    fin_input()
-    rs_part(1, 3, 0)
     s5(1, 1)
     late_outs(1)
     s3(1, 3)
+    rs2_ring_step(0, 1)
+    rs_part(1, 3, 2)
+    s4(1, 0)
+    rs_part(1, 3, 3)
+    rs_part(1, 3, 0)
     rs_part(1, 3, 1)
+    s5(1, 0)
+    late_outs(0)
+    rs2_ring_step(0, 2)
     s4(1, 2)
-    rs_last(1, 0)
+    rs_last(1, 2)
+    rs2_send(1, 2)
+    rs_last(1, 3)
+    rs2_send(1, 3)
     s5(1, 2)
     late_outs(2)
+    rs_last(1, 0)
+    rs2_send(1, 0)
+    s4(1, 3)
     rs_last(1, 1)
-    rs2_send(1)
-    s4(1, 3)
+    rs2_send(1, 1)
+    rs2_ring_step(0, 3)
     s5(1, 3)
+    late_outs(3)
+    fin_late()
+    turn_late(0)
+    turn_late(1)
+    turn_late(3)
     turn_late(2)
-    late_outs(3)
-    turn_late(1)
-    fin_late()
-    turn_late(3)
-    turn_late(0)
+    rs_out(0, True)
     rs_out(1, False)
     all_gone()
 
@@ -555,10 +620,10 @@
             pltpu.VMEM((2, 2, 8, 8, 32, 128), BF16),
             pltpu.VMEM((2, 128, 256), F32),
             dma((8,)), dma((2, 2)),
-            dma((2,)), dma((5,)),
-            dma((2, 2)), dma((2, 2, 4, 2)),
-            dma((2, 2)), dma((2, 2, 4, 2)),
-            dma((2,)), dma((5,)),
+            dma((2,)), dma((9,)),
+            dma((2, 2)), dma((2, 2, 4, 4)),
+            dma((2, 2)), dma((2, 2, 4, 4)),
+            dma((2,)), dma((9,)),
             dma((2, 4)), dma((2, 4)), dma((2, 4)), dma((2, 4)), dma((2, 4)),
         ],
         compiler_params=pltpu.CompilerParams(

time: 81.6 us -> 76.1 us (0.933)
  Pallas kernels: 80.8 us -> 75.3 us
    pallas_call x1, Pallas kernels: 79.7 us -> 74.2 us  [body(): pl.pallas_call(kernel, out_shape=tuple((pltpu.VMEM(shape, dtype) for shap...]
where the time goes in v3:
time: 76.1 us; the launch traced here: 75.9 us
  Pallas kernels  75.3 us (99%)
    pallas_call x1, Pallas kernels, body(): pl.pallas_call(kernel, out_shape=tuple((pltpu.VMEM(shape, dtype) for shap...  74.2 us

profile of v3, /device:TPU:1, one launch (start us, length us, event | category | flops | bytes accessed | tf_op | source)
XLA Modules:
  0.0 75.9 jit_solution(6806595618868429827)
XLA Ops:
  0.6 74.2 %shard_map.119 = (bf16[128,4096]{1,0:T(8,128)(2,1)S(1)}, bf16[128,256]{1,0:T(8,128)(2,1)S(1)}, bf16[128,256]{1,0:T(8,128)(2,1)S(1)}, f32[64,256]{1,0:T(8,128)S(1)}, f32[64,256]{1,0:T(8,128)S(1)}) custom-call(bf16[128,256]{1,0:T(8,128)(2,1)} %late_in_h.1, bf16[64,256]{1,0:T(8,128)(2,1)} %bitcast.5, bf16[64,256]{1,0:T(8,128)(2,1)} %down_h.1, ...), custom_call_target="tpu_custom_call" | custom-call | flops 1700000000 | bytes 8000000 | tf_op jit(solution)/shard_map/pallas_call | solution.py:595
  74.8 1.1 %shard_map.120 = (bf16[128,4096]{1,0:T(8,128)(2,1)}, bf16[128,256]{1,0:T(8,128)(2,1)}, bf16[128,256]{1,0:T(8,128)(2,1)}, f32[64,256]{1,0:T(8,128)}, f32[64,256]{1,0:T(8,128)}) custom-call(bf16[128,4096]{1,0:T(8,128)(2,1)S(1)} %get-tuple-element.15.refs_0_, bf16[128,256]{1,0:T(8,128)(2,1)S(1)} %get-tuple-element.16.refs_1_, ...), custom_call_target="tpu_custom_call" | custom-call | tf_op jit(solution)/shard_map/pallas_call | solution.py:639

commit v4 on v3

--- a/solution.py
+++ b/solution.py
@@ -64,16 +64,17 @@
         ).wait_send()
 
     barrier = pltpu.get_barrier_semaphore()
-    for axis, me, size in (("y", iy, 8), ("z", iz, 8), ("x", ix, 4), ("c", ic, 2)):
-        for step in range(1, size):
-            pl.semaphore_signal(
-                barrier, inc=1, device_id={axis: up_by(me, step, size)}, device_id_type=MESH
-            )
+    steps = [(step, axis, me, 8) for step in (4, 5, 3, 6, 2, 7, 1) for axis, me in (("z", iz), ("y", iy))]
+    steps += [(step, "x", ix, 4) for step in (2, 1, 3)] + [(1, "c", ic, 2)]
+    for step, axis, me, size in steps:
+        pl.semaphore_signal(
+            barrier, inc=1, device_id={axis: up_by(me, step, size)}, device_id_type=MESH
+        )
     loads = []
-    for at, (source, target) in enumerate((
-        (down_h, down), (up_t_h, up_t), (cot_h, cot), (late_in_h, late_in), (early_pre_h, early_pre),
-        (early_in_h, early_in), (down_sum_h, down_sum), (up_sum_h, up_sum),
-    )):
+    for at, source, target in (
+        (0, down_h, down), (1, cot_h, cot), (2, early_pre_h, early_pre), (3, up_t_h, up_t), (3, late_in_h, late_in),
+        (3, early_in_h, early_in), (3, down_sum_h, down_sum), (3, up_sum_h, up_sum),
+    ):
         copy = pltpu.make_async_copy(source, target, in_sem.at[at])
         copy.start()
         loads.append(copy)
@@ -92,25 +93,26 @@
 
         lax.fori_loop(8 * quarter, 8 * quarter + 8, one, 0)
 
+    loads[1].wait()
+    cot_t[...] = cot[...].T
     loads[2].wait()
-    cot_t[...] = cot[...].T
-    loads[4].wait()
     early(0)
     early(1)
     early(2)
     loads[0].wait()
     pl.semaphore_wait(barrier, 18)
 
-    own = []
-
     def own_copy(w):
         if w == 1:
-            loads[1].wait()
+            rest = weights.at[:, 1, pl.ds(0, 3), pl.ds(0, 3)]
+            pltpu.make_async_copy(rest, rest, in_sem.at[3]).wait()
         for h in range(2):
             rows = shards[w].at[pl.ds(32 * h, 32), :]
-            copy = pltpu.make_async_copy(rows, weights.at[w, h, place[h], 1], own_sem.at[w, h])
-            copy.start()
-            own.append(copy)
+            pltpu.make_async_copy(rows, weights.at[w, h, place[h], 1], own_sem.at[w]).start()
+
+    def own_wait(w):
+        both = weights.at[w, :, 0, 0]
+        pltpu.make_async_copy(both, both, own_sem.at[w]).wait()
 
     def others_in(part_at, parts):
         slots = range(part_at * 8 // parts, (part_at + 1) * 8 // parts)
@@ -127,8 +129,7 @@
 
     def ag1_wait(w, part_at):
         if part_at == 0:
-            for h in range(2):
-                own[2 * w + h].wait()
+            own_wait(w)
         count = len(others_in(part_at, GATHER_PARTS[w]))
         arrive(weights.at[w, 0, pl.ds(0, 2), pl.ds(0, count)], ag1_r.at[5 + part_at])
 
@@ -139,8 +140,8 @@
         send(ref, target, ag1_s.at[w], ag1_r.at[step], SUB_AXIS[h], up_by(sub_place[h], sign))
 
     def ag1_ring_start(w):
-        for h in range(2):
-            own[2 * w + h].wait()
+        own_wait(w)
+        for h in range(2):
             for way in range(2):
                 ring_send(w, h, way, 1)
 
@@ -155,7 +156,7 @@
         sign = 1 - 2 * way
         size = 8 // GATHER_PARTS[w]
         ref = weights.at[w, h, up_by(place[h], -sign * (step - 1)), pl.ds(size * part_at, size)]
-        send(ref, ref, ag2_s.at[w, h], ag2_r.at[w, h, step - 1, part_at], BLOCK_AXIS[h], up_by(place[h], sign))
+        send(ref, ref, ag2_s.at[w], ag2_r.at[w, step - 1, part_at], BLOCK_AXIS[h], up_by(place[h], sign))
 
     def ag2_start(w, part_at):
         for h in range(2):
@@ -165,8 +166,8 @@
     def ag2_part(w, step, part_at):
         parts = GATHER_PARTS[w]
         size = (16 if step < 4 else 8) // parts
-        for h in range(2):
-            arrive(weights.at[w, h, 0, pl.ds(0, size)], ag2_r.at[w, h, step - 1, part_at])
+        arrive(weights.at[w, :, 0, pl.ds(0, size)], ag2_r.at[w, step - 1, part_at])
+        for h in range(2):
             for way in range(2):
                 if step < 3 or (step == 3 and 2 * part_at // parts == way):
                     ag2_send(w, h, way, step + 1, part_at)
@@ -177,7 +178,7 @@
         send(
             grads.at[w, h, up_by(place[h], sign * (5 - step)), pl.ds(size * part_at, size)],
             ring_in.at[w, h, way, step - 1, pl.ds(size * part_at, size)],
-            rs1_s.at[w, h], rs1_r.at[w, h, step - 1, part_at], BLOCK_AXIS[h], up_by(place[h], sign),
+            rs1_s.at[w], rs1_r.at[w, step - 1, part_at], BLOCK_AXIS[h], up_by(place[h], sign),
         )
 
     def rs_start(w):
@@ -191,8 +192,8 @@
     def rs_part(w, step, part_at):
         parts = SCATTER_PARTS[w]
         size = 8 // parts
-        for h in range(2):
-            arrive(weights.at[w, h, 0, pl.ds(0, 2 * size if step > 1 else size)], rs1_r.at[w, h, step - 1, part_at])
+        arrive(weights.at[w, :, 0, pl.ds(0, 2 * size if step > 1 else size)], rs1_r.at[w, step - 1, part_at])
+        for h in range(2):
             for way in range(2):
                 if step == 1 and 2 * part_at // parts != way:
                     continue
@@ -204,8 +205,8 @@
 
     def rs_last(w, part_at):
         size = 8 // SCATTER_PARTS[w]
-        for h in range(2):
-            arrive(weights.at[w, h, 0, pl.ds(0, 2 * size)], rs1_r.at[w, h, 3, part_at])
+        arrive(weights.at[w, :, 0, pl.ds(0, 2 * size)], rs1_r.at[w, 3, part_at])
+        for h in range(2):
             mine = grads.at[w, h, place[h], pl.ds(size * part_at, size)]
             total = mine[...].astype(F32)
             for way in range(2):
@@ -282,7 +283,7 @@
     def s1(a, j):
         send(
             part.at[a, j, pl.ds(other_half, 512), :], pair_in.at[a, j],
-            tp_s.at[a, 0], pair_r.at[a, j], "c", other,
+            tp_s.at[a], pair_r.at[a, j], "c", other,
         )
 
     def s2(a, j):
@@ -293,7 +294,7 @@
         for step in (2, 1, 3):
             target = up_by(ix, step, 4)
             rows = pl.ds(pl.multiple_of(target * 128, 128), 128)
-            send(pair_sum.at[a, j, rows, :], x_in.at[a, j, step - 1], tp_s.at[a, 1], xr_r.at[a, j], "x", target)
+            send(pair_sum.at[a, j, rows, :], x_in.at[a, j, step - 1], tp_s.at[a], xr_r.at[a, j], "x", target)
 
     def share(a, core, x, j):
         return full.at[a, core, block_of(core, x // 2, j), pl.ds(4 * lax.rem(x, 2), 4)]
@@ -310,14 +311,14 @@
         ref = share(a, ic, ix, j)
         ref[...] = total.astype(BF16).reshape(4, 32, 128)
         for step in (2, 1, 3):
-            send(ref, ref, tp_s.at[a, 2], xg_r.at[a, j], "x", up_by(ix, step, 4))
-        send(ref, ref, tp_s.at[a, 3], fw_r.at[a, j], "c", other)
+            send(ref, ref, tp_s.at[a], xg_r.at[a, j], "x", up_by(ix, step, 4))
+        send(ref, ref, tp_s.at[a], fw_r.at[a, j], "c", other)
 
     def s4(a, j):
         arrive(x_in.at[a, j], xg_r.at[a, j])
         for step in (1, 2, 3):
             ref = share(a, ic, up_by(ix, step, 4), j)
-            send(ref, ref, tp_s.at[a, 3], fw_r.at[a, j], "c", other)
+            send(ref, ref, tp_s.at[a], fw_r.at[a, j], "c", other)
 
     def s5(a, j):
         arrive(pair_in.at[a, j], fw_r.at[a, j])
@@ -327,13 +328,9 @@
         for w in range(2):
             gone(small, ag1_s.at[w])
             gone(small, rs2_s.at[w])
-            for h in range(2):
-                gone(weights.at[w, h, pl.ds(0, 7)], ag2_s.at[w, h])
-                gone(weights.at[w, h, pl.ds(0, 7)], rs1_s.at[w, h])
-            gone(pair_in.at[w], tp_s.at[w, 0])
-            gone(x_in.at[w], tp_s.at[w, 1])
-            gone(x_in.at[w], tp_s.at[w, 2])
-            gone(pair_in.at[w], tp_s.at[w, 3])
+            gone(weights.at[w, :, pl.ds(0, 7)], ag2_s.at[w])
+            gone(weights.at[w, :, pl.ds(0, 7)], rs1_s.at[w])
+            gone(weights.at[w, :, pl.ds(0, 7)], tp_s.at[w])
 
     def pieces(j, fn):
         def one(at, _):
@@ -386,12 +383,8 @@
         pieces(j, fn)
 
     def prep_late():
-        loads[3].wait()
         late_t[...] = late_in[...].T
         acc[...] = jnp.zeros_like(acc)
-        loads[5].wait()
-        loads[6].wait()
-        loads[7].wait()
 
     def fin_late():
         late_out_o[...] = acc[1].astype(BF16)
@@ -401,180 +394,180 @@
 
     own_copy(0)
     ag1_send(0)
+    own_copy(1)
+    prep_late()
     early(3)
     down_grads(2)
     down_grads(0)
-    own_copy(1)
-    prep_late()
+    down_grads(3)
+    rs_start(0)
     down_grads(1)
-    down_grads(3)
     ag1_wait(0, 0)
+    ag2_start(0, 0)
     ag1_wait(0, 1)
-    ag2_start(0, 0)
     ag2_start(0, 1)
     ag1_ring_start(1)
+    ag1_wait(0, 3)
     ag1_wait(0, 2)
     ag2_start(0, 2)
-    ag1_wait(0, 3)
     ag2_start(0, 3)
     product(0, 0, (0,))
     ag2_part(0, 1, 0)
+    ag2_part(0, 1, 1)
     ag1_ring_step(1, 1)
     ag2_start(1, 0)
     ag2_part(0, 1, 2)
-    ag2_part(0, 1, 1)
     ag2_part(0, 1, 3)
     product(0, 0, (1,))
+    s1(0, 0)
     product(0, 1, (0,))
     ag2_part(0, 2, 0)
-    s1(0, 0)
+    ag2_part(0, 2, 1)
     ag1_ring_step(1, 2)
     ag2_start(1, 1)
-    ag2_part(1, 1, 0)
-    s2(0, 0)
     ag2_part(0, 2, 2)
-    ag2_part(0, 2, 1)
     ag2_part(0, 2, 3)
+    product(0, 2, (0,))
     product(0, 1, (1,))
     s1(0, 1)
-    product(0, 2, (0,))
-    ag2_part(0, 3, 0)
+    ag2_part(1, 1, 0)
+    ag2_part(0, 3, 1)
     ag1_ring_step(1, 3)
     s2(0, 1)
-    ag2_part(1, 2, 0)
-    ag2_start(1, 3)
-    s3(0, 0)
+    s2(0, 0)
+    ag2_part(1, 1, 1)
     ag2_part(0, 3, 2)
-    ag2_part(0, 3, 1)
     ag2_part(0, 3, 3)
+    ag2_part(0, 3, 0)
+    product(0, 3, (0,))
     product(0, 2, (1,))
     s1(0, 2)
-    ag2_part(1, 1, 1)
-    product(0, 3, (0,))
-    ag2_part(0, 4, 0)
+    ag2_start(1, 3)
+    ag2_part(1, 2, 0)
+    ag2_part(0, 4, 1)
     ag1_ring_step(1, 4)
     ag2_start(1, 2)
     product(1, 0, (0,))
-    ag2_part(1, 3, 0)
     s2(0, 2)
-    s3(0, 1)
-    ag2_part(1, 1, 3)
     ag2_part(0, 4, 2)
-    ag2_part(0, 4, 1)
-    rs_start(0)
     ag2_part(0, 4, 3)
+    ag2_part(0, 4, 0)
     product(0, 3, (1,))
     s1(0, 3)
+    s3(0, 0)
     ag2_part(1, 2, 1)
-    s4(0, 0)
+    rs_part(0, 1, 3)
+    rs_part(0, 1, 2)
+    rs_part(0, 1, 0)
+    s2(0, 3)
+    ag2_part(1, 1, 3)
     ag2_part(1, 1, 2)
     product(1, 0, (1,))
+    product(1, 1, (0,))
     s1(1, 0)
-    s2(0, 3)
-    product(1, 1, (0,))
-    ag2_part(1, 4, 0)
+    s3(0, 2)
+    ag2_part(1, 3, 0)
+    rs_part(0, 1, 1)
+    rs_part(0, 2, 3)
+    s4(0, 0)
+    rs_part(0, 2, 0)
+    rs_part(0, 2, 2)
+    ag2_part(1, 2, 3)
+    s3(0, 3)
     s5(0, 0)
     up_grads(0)
-    ag2_part(1, 2, 3)
-    s3(0, 2)
-    rs_part(0, 1, 2)
-    rs_part(0, 1, 0)
-    rs_part(0, 1, 3)
-    rs_part(0, 1, 1)
-    s4(0, 1)
+    ag2_part(1, 2, 2)
+    product(1, 2, (0,))
+    product(1, 1, (1,))
+    s1(1, 1)
+    s4(0, 2)
+    rs_part(0, 2, 1)
+    s3(0, 1)
+    ag2_part(1, 4, 0)
     ag2_part(1, 3, 1)
-    s5(0, 1)
-    up_grads(1)
-    ag2_part(1, 2, 2)
-    s3(0, 3)
-    product(1, 1, (1,))
-    ag2_part(1, 3, 3)
-    s1(1, 1)
-    product(1, 2, (0,))
-    rs_part(0, 2, 2)
-    rs_part(0, 2, 3)
-    rs_part(0, 2, 1)
+    s2(1, 0)
+    rs_part(0, 3, 3)
     s2(1, 1)
-    s4(0, 2)
-    ag2_part(1, 4, 1)
-    rs_part(0, 2, 0)
-    ag2_part(1, 3, 2)
-    product(1, 2, (1,))
-    product(1, 3, (0,))
+    rs_part(0, 3, 0)
     s5(0, 2)
     up_grads(2)
     rs_part(0, 3, 2)
-    s1(1, 2)
-    ag2_part(1, 4, 3)
-    s2(1, 0)
     s4(0, 3)
-    rs_part(0, 3, 3)
-    s2(1, 2)
-    rs_part(0, 3, 1)
+    ag2_part(1, 3, 3)
+    ag2_part(1, 3, 2)
+    product(1, 3, (0,))
+    product(1, 2, (1,))
     s5(0, 3)
     up_grads(3)
     rs_start(1)
-    rs_part(0, 3, 0)
+    s1(1, 2)
+    rs_part(0, 3, 1)
+    s4(0, 1)
+    ag2_part(1, 4, 1)
+    s3(1, 0)
+    rs_last(0, 3)
+    rs_last(0, 0)
+    s2(1, 2)
+    s5(0, 1)
+    up_grads(1)
+    rs_last(0, 2)
+    ag2_part(1, 4, 3)
+    ag2_part(1, 4, 2)
+    input_grads(1)
+    rs_part(1, 1, 2)
     s3(1, 1)
-    ag2_part(1, 4, 2)
+    rs_part(1, 1, 1)
+    input_grads(3)
+    rs_part(1, 1, 3)
     product(1, 3, (1,))
-    input_grads(3)
     s1(1, 3)
+    rs_part(1, 1, 0)
+    input_grads(2)
+    s4(1, 0)
     input_grads(0)
-    rs_last(0, 2)
-    input_grads(2)
+    s2(1, 3)
+    s3(1, 2)
     rs_last(0, 1)
-    rs_part(1, 1, 2)
-    s2(1, 3)
-    rs_last(0, 3)
-    input_grads(1)
+    rs2_ring_start(0)
     fin_input()
-    rs_part(1, 1, 3)
-    rs_part(1, 1, 0)
-    s3(1, 0)
-    s3(1, 2)
-    rs_part(1, 1, 1)
-    rs_last(0, 0)
-    rs2_ring_start(0)
     rs_part(1, 2, 2)
+    s5(1, 0)
+    late_outs(0)
+    rs_part(1, 2, 3)
     s4(1, 1)
-    rs_part(1, 2, 3)
     rs_part(1, 2, 0)
     rs_part(1, 2, 1)
     s5(1, 1)
     late_outs(1)
-    s3(1, 3)
     rs2_ring_step(0, 1)
     rs_part(1, 3, 2)
-    s4(1, 0)
+    s3(1, 3)
     rs_part(1, 3, 3)
     rs_part(1, 3, 0)
+    s4(1, 2)
     rs_part(1, 3, 1)
-    s5(1, 0)
-    late_outs(0)
     rs2_ring_step(0, 2)
-    s4(1, 2)
+    s5(1, 2)
+    late_outs(2)
     rs_last(1, 2)
     rs2_send(1, 2)
     rs_last(1, 3)
     rs2_send(1, 3)
-    s5(1, 2)
-    late_outs(2)
+    s4(1, 3)
     rs_last(1, 0)
     rs2_send(1, 0)
-    s4(1, 3)
     rs_last(1, 1)
     rs2_send(1, 1)
+    s5(1, 3)
+    turn_late(2)
     rs2_ring_step(0, 3)
-    s5(1, 3)
+    turn_late(0)
     late_outs(3)
     fin_late()
-    turn_late(0)
     turn_late(1)
     turn_late(3)
-    turn_late(2)
+    rs_out(1, False)
     rs_out(0, True)
-    rs_out(1, False)
     all_gone()
 
 
@@ -619,12 +612,12 @@
             pltpu.VMEM((2, 4, 3, 128, 128), BF16),
             pltpu.VMEM((2, 2, 8, 8, 32, 128), BF16),
             pltpu.VMEM((2, 128, 256), F32),
-            dma((8,)), dma((2, 2)),
+            dma((4,)), dma((2,)),
             dma((2,)), dma((9,)),
-            dma((2, 2)), dma((2, 2, 4, 4)),
-            dma((2, 2)), dma((2, 2, 4, 4)),
+            dma((2,)), dma((2, 4, 4)),
+            dma((2,)), dma((2, 4, 4)),
             dma((2,)), dma((9,)),
-            dma((2, 4)), dma((2, 4)), dma((2, 4)), dma((2, 4)), dma((2, 4)),
+            dma((2,)), dma((2, 4)), dma((2, 4)), dma((2, 4)), dma((2, 4)),
         ],
         compiler_params=pltpu.CompilerParams(
             collective_id=0, has_side_effects=True, vmem_limit_bytes=36 * 1024 * 1024

time: 76.1 us -> 75.3 us (0.989)
  Pallas kernels: 75.3 us -> 74.5 us
    pallas_call x1, Pallas kernels: 74.2 us -> 73.4 us  [body(): pl.pallas_call(kernel, out_shape=tuple((pltpu.VMEM(shape, dtype) for shap...]
where the time goes in v4:
time: 75.3 us; the launch traced here: 75.1 us
  Pallas kernels  74.5 us (99%)
    pallas_call x1, Pallas kernels, body(): pl.pallas_call(kernel, out_shape=tuple((pltpu.VMEM(shape, dtype) for shap...  73.4 us

profile of v4, /device:TPU:1, one launch (start us, length us, event | category | flops | bytes accessed | tf_op | source)
XLA Modules:
  0.0 75.1 jit_solution(12538782895658686206)
XLA Ops:
  0.6 73.4 %shard_map.119 = (bf16[128,4096]{1,0:T(8,128)(2,1)S(1)}, bf16[128,256]{1,0:T(8,128)(2,1)S(1)}, bf16[128,256]{1,0:T(8,128)(2,1)S(1)}, f32[64,256]{1,0:T(8,128)S(1)}, f32[64,256]{1,0:T(8,128)S(1)}) custom-call(bf16[128,256]{1,0:T(8,128)(2,1)} %late_in_h.1, bf16[64,256]{1,0:T(8,128)(2,1)} %bitcast.5, bf16[64,256]{1,0:T(8,128)(2,1)} %down_h.1, ...), custom_call_target="tpu_custom_call" | custom-call | flops 1700000000 | bytes 8000000 | tf_op jit(solution)/shard_map/pallas_call | solution.py:588
  74.0 1.1 %shard_map.120 = (bf16[128,4096]{1,0:T(8,128)(2,1)}, bf16[128,256]{1,0:T(8,128)(2,1)}, bf16[128,256]{1,0:T(8,128)(2,1)}, f32[64,256]{1,0:T(8,128)}, f32[64,256]{1,0:T(8,128)}) custom-call(bf16[128,4096]{1,0:T(8,128)(2,1)S(1)} %get-tuple-element.15.refs_0_, bf16[128,256]{1,0:T(8,128)(2,1)S(1)} %get-tuple-element.16.refs_1_, ...), custom_call_target="tpu_custom_call" | custom-call | tf_op jit(solution)/shard_map/pallas_call | solution.py:632

commit v5 on v4

--- a/solution.py
+++ b/solution.py
@@ -394,13 +394,13 @@
 
     own_copy(0)
     ag1_send(0)
+    early(3)
+    down_grads(3)
+    down_grads(2)
     own_copy(1)
+    rs_start(0)
+    down_grads(0)
     prep_late()
-    early(3)
-    down_grads(2)
-    down_grads(0)
-    down_grads(3)
-    rs_start(0)
     down_grads(1)
     ag1_wait(0, 0)
     ag2_start(0, 0)
@@ -418,135 +418,136 @@
     ag2_start(1, 0)
     ag2_part(0, 1, 2)
     ag2_part(0, 1, 3)
+    product(0, 1, (0,))
     product(0, 0, (1,))
     s1(0, 0)
-    product(0, 1, (0,))
     ag2_part(0, 2, 0)
     ag2_part(0, 2, 1)
     ag1_ring_step(1, 2)
     ag2_start(1, 1)
+    s2(0, 0)
     ag2_part(0, 2, 2)
     ag2_part(0, 2, 3)
+    product(0, 1, (1,))
     product(0, 2, (0,))
-    product(0, 1, (1,))
     s1(0, 1)
     ag2_part(1, 1, 0)
     ag2_part(0, 3, 1)
+    s2(0, 1)
     ag1_ring_step(1, 3)
-    s2(0, 1)
-    s2(0, 0)
     ag2_part(1, 1, 1)
     ag2_part(0, 3, 2)
+    s3(0, 0)
+    ag2_part(0, 3, 0)
     ag2_part(0, 3, 3)
-    ag2_part(0, 3, 0)
+    product(0, 2, (1,))
     product(0, 3, (0,))
-    product(0, 2, (1,))
+    ag2_part(1, 2, 0)
     s1(0, 2)
-    ag2_start(1, 3)
-    ag2_part(1, 2, 0)
     ag2_part(0, 4, 1)
     ag1_ring_step(1, 4)
     ag2_start(1, 2)
+    ag2_start(1, 3)
     product(1, 0, (0,))
     s2(0, 2)
+    s3(0, 1)
+    ag2_part(1, 2, 1)
     ag2_part(0, 4, 2)
+    ag2_part(0, 4, 0)
     ag2_part(0, 4, 3)
-    ag2_part(0, 4, 0)
+    rs_part(0, 1, 1)
+    rs_part(0, 1, 2)
     product(0, 3, (1,))
     s1(0, 3)
-    s3(0, 0)
-    ag2_part(1, 2, 1)
     rs_part(0, 1, 3)
-    rs_part(0, 1, 2)
+    s4(0, 0)
+    ag2_part(1, 3, 0)
     rs_part(0, 1, 0)
     s2(0, 3)
-    ag2_part(1, 1, 3)
     ag2_part(1, 1, 2)
-    product(1, 0, (1,))
-    product(1, 1, (0,))
-    s1(1, 0)
-    s3(0, 2)
-    ag2_part(1, 3, 0)
-    rs_part(0, 1, 1)
-    rs_part(0, 2, 3)
-    s4(0, 0)
-    rs_part(0, 2, 0)
-    rs_part(0, 2, 2)
-    ag2_part(1, 2, 3)
-    s3(0, 3)
     s5(0, 0)
     up_grads(0)
+    ag2_part(1, 1, 3)
+    product(1, 0, (1,))
+    s1(1, 0)
+    product(1, 1, (0,))
+    s3(0, 2)
+    rs_part(0, 2, 1)
+    rs_part(0, 2, 2)
+    s4(0, 1)
+    s2(1, 0)
+    ag2_part(1, 4, 0)
+    rs_part(0, 2, 3)
+    rs_part(0, 2, 0)
+    s5(0, 1)
+    up_grads(1)
+    s3(0, 3)
     ag2_part(1, 2, 2)
+    ag2_part(1, 2, 3)
     product(1, 2, (0,))
     product(1, 1, (1,))
+    rs_part(0, 3, 1)
     s1(1, 1)
     s4(0, 2)
-    rs_part(0, 2, 1)
-    s3(0, 1)
-    ag2_part(1, 4, 0)
     ag2_part(1, 3, 1)
-    s2(1, 0)
+    rs_part(0, 3, 2)
+    s2(1, 1)
     rs_part(0, 3, 3)
-    s2(1, 1)
-    rs_part(0, 3, 0)
     s5(0, 2)
     up_grads(2)
-    rs_part(0, 3, 2)
+    s3(1, 0)
+    rs_part(0, 3, 0)
+    ag2_part(1, 3, 2)
     s4(0, 3)
     ag2_part(1, 3, 3)
-    ag2_part(1, 3, 2)
     product(1, 3, (0,))
     product(1, 2, (1,))
+    s1(1, 2)
+    rs_last(0, 1)
     s5(0, 3)
     up_grads(3)
+    ag2_part(1, 4, 1)
     rs_start(1)
-    s1(1, 2)
-    rs_part(0, 3, 1)
-    s4(0, 1)
-    ag2_part(1, 4, 1)
-    s3(1, 0)
+    s3(1, 1)
+    rs_last(0, 2)
+    s2(1, 2)
     rs_last(0, 3)
+    s4(1, 0)
+    ag2_part(1, 4, 2)
     rs_last(0, 0)
-    s2(1, 2)
-    s5(0, 1)
-    up_grads(1)
-    rs_last(0, 2)
+    rs2_ring_start(0)
     ag2_part(1, 4, 3)
-    ag2_part(1, 4, 2)
-    input_grads(1)
-    rs_part(1, 1, 2)
-    s3(1, 1)
-    rs_part(1, 1, 1)
-    input_grads(3)
-    rs_part(1, 1, 3)
     product(1, 3, (1,))
     s1(1, 3)
+    input_grads(1)
+    s5(1, 0)
+    rs_part(1, 1, 2)
+    late_outs(0)
+    rs_part(1, 1, 3)
     rs_part(1, 1, 0)
-    input_grads(2)
-    s4(1, 0)
+    rs_part(1, 1, 1)
     input_grads(0)
+    s4(1, 1)
+    input_grads(3)
+    rs2_ring_step(0, 1)
     s2(1, 3)
     s3(1, 2)
-    rs_last(0, 1)
-    rs2_ring_start(0)
-    fin_input()
+    input_grads(2)
     rs_part(1, 2, 2)
-    s5(1, 0)
-    late_outs(0)
-    rs_part(1, 2, 3)
-    s4(1, 1)
-    rs_part(1, 2, 0)
-    rs_part(1, 2, 1)
     s5(1, 1)
     late_outs(1)
-    rs2_ring_step(0, 1)
+    rs_part(1, 2, 3)
+    fin_input()
+    rs_part(1, 2, 1)
+    rs2_ring_step(0, 2)
+    rs_part(1, 2, 0)
     rs_part(1, 3, 2)
     s3(1, 3)
     rs_part(1, 3, 3)
-    rs_part(1, 3, 0)
     s4(1, 2)
     rs_part(1, 3, 1)
-    rs2_ring_step(0, 2)
+    rs2_ring_step(0, 3)
+    rs_part(1, 3, 0)
     s5(1, 2)
     late_outs(2)
     rs_last(1, 2)
@@ -554,20 +555,19 @@
     rs_last(1, 3)
     rs2_send(1, 3)
     s4(1, 3)
+    rs_last(1, 1)
+    rs2_send(1, 1)
+    rs_out(0, True)
+    s5(1, 3)
+    turn_late(1)
     rs_last(1, 0)
     rs2_send(1, 0)
-    rs_last(1, 1)
-    rs2_send(1, 1)
-    s5(1, 3)
+    turn_late(3)
     turn_late(2)
-    rs2_ring_step(0, 3)
-    turn_late(0)
     late_outs(3)
     fin_late()
-    turn_late(1)
-    turn_late(3)
+    turn_late(0)
     rs_out(1, False)
-    rs_out(0, True)
     all_gone()
 
 

time: 75.3 us -> 74.6 us (level)
  no operation moved by 1% of the time
where the time goes in v5:
time: 74.6 us; the launch traced here: 74.5 us
  Pallas kernels  73.9 us (99%)
    pallas_call x1, Pallas kernels, body(): pl.pallas_call(kernel, out_shape=tuple((pltpu.VMEM(shape, dtype) for shap...  72.8 us

profile of v5, /device:TPU:1, one launch (start us, length us, event | category | flops | bytes accessed | tf_op | source)
XLA Modules:
  0.0 74.5 jit_solution(3384090209241335737)
XLA Ops:
  0.6 72.8 %shard_map.119 = (bf16[128,4096]{1,0:T(8,128)(2,1)S(1)}, bf16[128,256]{1,0:T(8,128)(2,1)S(1)}, bf16[128,256]{1,0:T(8,128)(2,1)S(1)}, f32[64,256]{1,0:T(8,128)S(1)}, f32[64,256]{1,0:T(8,128)S(1)}) custom-call(bf16[128,256]{1,0:T(8,128)(2,1)} %late_in_h.1, bf16[64,256]{1,0:T(8,128)(2,1)} %bitcast.5, bf16[64,256]{1,0:T(8,128)(2,1)} %down_h.1, ...), custom_call_target="tpu_custom_call" | custom-call | flops 1700000000 | bytes 8000000 | tf_op jit(solution)/shard_map/pallas_call | solution.py:588
  73.4 1.1 %shard_map.120 = (bf16[128,4096]{1,0:T(8,128)(2,1)}, bf16[128,256]{1,0:T(8,128)(2,1)}, bf16[128,256]{1,0:T(8,128)(2,1)}, f32[64,256]{1,0:T(8,128)}, f32[64,256]{1,0:T(8,128)}) custom-call(bf16[128,4096]{1,0:T(8,128)(2,1)S(1)} %get-tuple-element.15.refs_0_, bf16[128,256]{1,0:T(8,128)(2,1)S(1)} %get-tuple-element.16.refs_1_, ...), custom_call_target="tpu_custom_call" | custom-call | tf_op jit(solution)/shard_map/pallas_call | solution.py:632
